TPU v7x, 512 devices: a whole 4x8x8 slice. The times are simulated.
512 devices in a mesh: sp: 32 (over z, x), dp: 16 (over y, core).
Axes of the slice: x: 4, y: 8, z: 8, core: 2. Of those that a mesh axis runs over, the one named last changes fastest.
Arguments:
- tokens: bfloat16 [128, 2048, 2048], P('dp', 'sp'), may hold values from -6 to 6
- pre_gain: float32 [2048], replicated, may hold values from 0.1 to 1.9
- w_query: bfloat16 [2048, 512], P('dp'), may hold values from -0.125 to 0.125
- w_forget: bfloat16 [2048, 512], P('dp'), may hold values from -0.125 to 0.125
- w_value: bfloat16 [2048, 512], P('dp'), may hold values from -0.125 to 0.125
- w_gate: bfloat16 [2048, 512], P('dp'), may hold values from -0.125 to 0.125
- lower_bound: float32 [512], replicated, may hold values from 0.8 to 1
- extra_decay: float32 [512, 2048], P(('dp', 'sp')), may hold values from -1.5 to 0
- initial_state: float32 [512, 128, 128], P(('dp', 'sp')), may hold values from -0.18 to 0.18
- norm_gain: float32 [128], replicated, may hold values from 0.1 to 1.9
- w_out: bfloat16 [512, 2048], P('dp'), may hold values from -0.25 to 0.25
- post_gain: float32 [2048], replicated, may hold values from 0.1 to 1.9
Outputs:
- layer_out: bfloat16 [128, 2048, 2048], P('dp', 'sp')
All inputs are finite; a program needn't handle non-finite values.
Results may differ from a plain program's by a relative error of at most 0.015.
Values may be sent and summed in bfloat16 or wider, within the bound.
No kernel may reach another device: no remote copies, remote signals or barrier semaphores. Data moves between devices by JAX's collectives and lax.ppermute only.
A program may use at most 64 MiB of HBM per device.

v0:
```python
import jax
import jax.numpy as jnp
from jax import lax
from jax.experimental import pallas as pl
from jax.experimental.pallas import tpu as pltpu
from jax.sharding import Mesh
from jax.sharding import PartitionSpec as P


HEADS = 4
HK = 128
HV = 128
CHUNK = 64
PAIR = 2 * CHUNK
TAIL = 8
SP = ("z", "x")
DP = ("y", "c")
DP_SP = ("y", "c", "z", "x")
OFFSETS = (0, -1, 1, -2, 2, -3, 3, 4)
ROWS = 128
OUT_ROWS = 32
EPS = 1e-06


F32 = jnp.float32
BF16 = jnp.bfloat16


def shifted(a, step):
    size = lax.axis_size("y")
    return lax.ppermute(a, "y", [(i, (i + step) % size) for i in range(size)])


def swapped(a):
    return lax.ppermute(a, "c", [(0, 1), (1, 0)])


def after(values, others):
    return lax.optimization_barrier((*values, *others))[: len(values)]


def gathered_y(shard, waits):
    pieces = [shard]
    up = down = shard
    for k in range(3):
        up, down = after((up, down), waits[k]) if waits[k] else (up, down)
        up, down = shifted(up, 1), shifted(down, -1)
        pieces += [up, down]
    up, down = after((up, down), waits[3]) if waits[3] else (up, down)
    half = shard.shape[0] // 2
    up, down = up[:half], down[half:]
    pieces += [shifted(up, 1), shifted(down, -1)]
    return stacked_pieces(pieces)


def stack_kernel(*refs):
    out_ref = refs[-1]
    first = 0
    for ref in refs[:-1]:
        rows = ref.shape[0]
        out_ref[first : first + rows, :] = ref[...]
        first += rows


def stacked_pieces(pieces):
    rows = sum(p.shape[0] for p in pieces)
    return pl.pallas_call(
        stack_kernel,
        in_specs=[vmem_spec()] * len(pieces),
        out_specs=vmem_spec(),
        out_shape=jax.ShapeDtypeStruct((rows, pieces[0].shape[1]), BF16),
        compiler_params=limit(8),
        name="stack",
    )(*pieces)


def dot(a, b):
    return jnp.dot(a, b, preferred_element_type=F32)


def dot_nt(a, b):
    return lax.dot_general(a, b, (((1,), (1,)), ((), ())), preferred_element_type=F32)


def dot_tn(a, b):
    return lax.dot_general(a, b, (((0,), (0,)), ((), ())), preferred_element_type=F32)


def sigmoid(a):
    return 0.5 * jnp.tanh(0.5 * a) + 0.5


def place(where_ref, j):
    core = where_ref[1] if j < len(OFFSETS) else 1 - where_ref[1]
    return 2 * ((where_ref[0] + OFFSETS[j % len(OFFSETS)] + 8) & 7) + core


def norm_kernel(where_ref, x_ref, gain_ref, out_ref):
    x = x_ref[...].astype(F32)
    scale = lax.rsqrt(jnp.mean(x * x, axis=-1, keepdims=True) + EPS)
    rows = pl.ds(pl.multiple_of(pl.program_id(0) * x.shape[0], x.shape[0]), x.shape[0])
    for j in range(2 * len(OFFSETS)):
        start = pl.multiple_of(place(where_ref, j) * ROWS, ROWS)
        part = x_ref[:, pl.ds(start, ROWS)].astype(F32) * scale * gain_ref[:, pl.ds(start, ROWS)]
        out_ref[rows, j * ROWS : (j + 1) * ROWS] = part.astype(BF16)


def normed_tokens(tokens, pre_gain, where):
    rows, width = tokens.shape
    tile = 128
    return pl.pallas_call(
        norm_kernel,
        grid_spec=pltpu.PrefetchScalarGridSpec(
            num_scalar_prefetch=1,
            grid=(rows // tile,),
            in_specs=[
                pl.BlockSpec((tile, width), lambda i, b: (i, 0)),
                pl.BlockSpec((1, width), lambda i, b: (0, 0)),
            ],
            out_specs=pl.BlockSpec(memory_space=pltpu.VMEM),
        ),
        out_shape=jax.ShapeDtypeStruct((rows, width), BF16),
        compiler_params=pltpu.CompilerParams(vmem_limit_bytes=6 << 20),
        name="norm",
    )(where, tokens, pre_gain.reshape(1, width))


def vmem_spec():
    return pl.BlockSpec(memory_space=pltpu.VMEM)


def limit(mib):
    return pltpu.CompilerParams(vmem_limit_bytes=mib << 20)


def project_kernel(a_ref, own_ref, other_ref, out_ref):
    half = own_ref.shape[0]
    seqs, heads, _, local_len, _ = out_ref.shape
    wide = heads * HK
    cols = pl.ds(pl.multiple_of(pl.program_id(0) * wide, wide), wide)
    total = dot(a_ref[:, :half], own_ref[:, cols]) + dot(a_ref[:, half:], other_ref[:, cols])
    total = total.astype(BF16)
    for n in range(heads):
        out_ref[:, n, 0] = total[:, n * HK : (n + 1) * HK].reshape(seqs, local_len, HK)


def project_heads(normed, own, other, seqs, local_len):
    block = (seqs, 2, 1, local_len, HK)
    return pl.pallas_call(
        project_kernel,
        grid=(HEADS,),
        in_specs=[vmem_spec()] * 3,
        out_specs=pl.BlockSpec(block, lambda j: (0, j % 2, j // 2, 0, 0)),
        out_shape=pltpu.HBM((seqs, HEADS, 2, local_len, HK), BF16),
        compiler_params=limit(8),
        name="project",
    )(normed, own, other)


def pair_masks():
    row = lax.broadcasted_iota(jnp.int32, (PAIR, PAIR), 0)
    col = lax.broadcasted_iota(jnp.int32, (PAIR, PAIR), 1)
    causal = (row >= col) & ((row < CHUNK) == (col < CHUNK))
    return causal, row < CHUNK, col < CHUNK


def keys_and_total(f, gap, ones):
    keys = gap * sigmoid(-f)
    decay = jnp.log1p(-keys)
    high = decay.astype(BF16)
    low = (decay - high.astype(F32)).astype(BF16)
    return keys, dot(ones, high) + dot(ones, low)


def state_kernel(fv_ref, run_ref, tail_ref, gap_ref, state_ref, out_ref, carry_ref):
    chunks = out_ref.shape[0]
    causal, first_row, _ = pair_masks()
    ones = causal.astype(F32).astype(BF16)
    gap = gap_ref[...]
    block = pl.program_id(0)

    @pl.when(block == 0)
    def _():
        carry_ref[...] = state_ref[...]

    state = carry_ref[...]
    for p in range(chunks // 2):
        b = block * chunks + 2 * p
        f = fv_ref[pl.ds(b, 2), 0].reshape(PAIR, HK).astype(F32)
        keys, total = keys_and_total(f, gap, ones)
        run_row = run_ref[pl.ds(block * (chunks // 2) + p, 1), :]
        run = jnp.broadcast_to(run_row, (PAIR, PAIR)).T
        ends = [total[n * CHUNK + CHUNK - 1 : (n + 1) * CHUNK, :] for n in range(2)]
        run_ends = [run[n * CHUNK + CHUNK - 1 : (n + 1) * CHUNK, :] for n in range(2)]
        end = jnp.where(first_row, ends[0], ends[1])
        run_end = jnp.where(first_row, run_ends[0], run_ends[1])
        weighted = (keys * jnp.exp((end - total) + (run_end - run))).astype(BF16)
        for n in range(2):
            out_ref[2 * p + n, 0:HV, :] = state.astype(BF16)
            out_ref[2 * p + n, HV:, :] = tail_ref[b + n]
            rows = slice(n * CHUNK, (n + 1) * CHUNK)
            added = dot_tn(fv_ref[b + n, 1], weighted[rows])
            state = state * jnp.exp(ends[n] + run_ends[n]) + added
    carry_ref[...] = state


def chunk_states(fv, run, tail, gap, state):
    chunks = fv.shape[0]
    group = 8
    return pl.pallas_call(
        state_kernel,
        grid=(chunks // group,),
        in_specs=[
            vmem_spec(),
            pl.BlockSpec(run.shape, lambda i: (0, 0)),
            pl.BlockSpec(tail.shape, lambda i: (0, 0, 0)),
            pl.BlockSpec(gap.shape, lambda i: (0, 0)),
            pl.BlockSpec(state.shape, lambda i: (0, 0)),
        ],
        out_specs=pl.BlockSpec((group, HV + TAIL, HK), lambda i: (i, 0, 0)),
        out_shape=pltpu.HBM((chunks, HV + TAIL, HK), BF16),
        scratch_shapes=[pltpu.VMEM((HV, HK), F32)],
        compiler_params=limit(6),
        name="state",
    )(fv, run, tail, gap, state)


def local_kernel(a_ref, own_ref, other_ref, fv_ref, gap_ref, out_ref):
    half = own_ref.shape[0]
    seqs, heads, _, _, _ = fv_ref.shape
    wide = heads * HK
    causal, _, _ = pair_masks()
    ones = causal.astype(F32).astype(BF16)
    total_q = dot(a_ref[:, :half], own_ref[:, :wide]) + dot(a_ref[:, half:], other_ref[:, :wide])
    q_pre = total_q.astype(BF16)
    total_g = dot(a_ref[:, :half], own_ref[:, wide : 2 * wide])
    total_g += dot(a_ref[:, half:], other_ref[:, wide : 2 * wide])
    g_pre = total_g.astype(BF16)
    for p in range(seqs // 2):
        for h in range(heads):
            q = q_pre[p * PAIR : (p + 1) * PAIR, h * HK : (h + 1) * HK].astype(F32)
            f = fv_ref[2 * p : 2 * p + 2, h, 0].reshape(PAIR, HK).astype(F32)
            keys, total = keys_and_total(f, gap_ref[h : h + 1, :], ones)
            q_scaled = (q * sigmoid(q) * jnp.exp(total)).astype(BF16)
            k_scaled = (keys * jnp.exp(-total)).astype(BF16)
            out_ref[0, p, h] = q_scaled
            out_ref[1, p, h] = jnp.where(causal, dot_nt(q_scaled, k_scaled), 0.0).astype(BF16)
            out_ref[2, p, h] = g_pre[p * PAIR : (p + 1) * PAIR, h * HV : (h + 1) * HV]


def weight_kernel(where_ref, own_ref, other_ref, weight_ref):
    wide = HEADS * HV
    for k, stack in enumerate((own_ref, other_ref)):
        for j in range(len(OFFSETS)):
            start = pl.multiple_of(place(where_ref, k * len(OFFSETS) + j) * OUT_ROWS, OUT_ROWS)
            for n in range(ROWS // OUT_ROWS):
                first = j * ROWS + n * OUT_ROWS
                weight_ref[pl.ds(start, OUT_ROWS), n * wide : (n + 1) * wide] = stack[
                    first : first + OUT_ROWS, 2 * wide :
                ]


def local_parts(normed, own, other, fv, gap):
    seqs, heads, _, _, _ = fv.shape
    return pl.pallas_call(
        local_kernel,
        in_specs=[vmem_spec()] * 5,
        out_shape=pltpu.HBM((3, seqs // 2, heads, PAIR, HK), BF16),
        compiler_params=limit(14),
        name="local",
    )(normed, own, other, fv, gap)


def out_weight(where, own, other, width):
    return pl.pallas_call(
        weight_kernel,
        in_specs=[pl.BlockSpec(memory_space=pltpu.SMEM)] + [vmem_spec()] * 2,
        out_specs=vmem_spec(),
        out_shape=jax.ShapeDtypeStruct((HEADS * HV, width), BF16),
        compiler_params=limit(4),
        name="weight",
    )(where, own, other)


def output_kernel(state_ref, part_ref, fv_ref, weight_ref, norm_ref, post_ref, out_ref):
    heads = fv_ref.shape[1]
    pairs = out_ref.shape[0] // 2
    _, _, first_col = pair_masks()
    gain = norm_ref[...]
    rows = []
    for n_pair in range(pairs):
        p = n_pair
        gated = []
        for h in range(heads):
            runs, carried = [], []
            for n in range(2):
                s = pl.program_id(0) * 2 * pairs + 2 * p + n
                tail = state_ref[s, h, HV:, :].astype(F32)
                runs.append(tail[0:1, :] + tail[1:2, :] + tail[2:3, :])
                query = part_ref[0, p, h, n * CHUNK : (n + 1) * CHUNK, :]
                carried.append(dot_nt(query, state_ref[s, h, 0:HV, :]))
            run = jnp.where(first_col, runs[0], runs[1])
            run_cols = run.T
            weight = jnp.exp(jnp.minimum(run_cols - run, 0.0))
            scores = (part_ref[1, p, h].astype(F32) * weight).astype(BF16)
            v = fv_ref[2 * p : 2 * p + 2, h, 0].reshape(PAIR, HV)
            out = jnp.concatenate(carried, axis=0) * jnp.exp(run_cols) + dot(scores, v)
            scale = lax.rsqrt(jnp.mean(out * out, axis=-1, keepdims=True) + EPS)
            head = (out * scale * gain).astype(BF16).astype(F32)
            gate = part_ref[2, p, h].astype(F32)
            gated.append((head * (gate * sigmoid(gate))).astype(BF16))
        rows.append(jnp.concatenate(gated, axis=1))
    mixed = dot(jnp.concatenate(rows, axis=0), weight_ref[...])
    scale = lax.rsqrt(jnp.mean(mixed * mixed, axis=-1, keepdims=True) + EPS)
    out_ref[...] = (mixed * scale * post_ref[...]).astype(BF16).reshape(out_ref.shape)


def output_rows(states, parts, fv, weight, norm_gain, post_gain):
    seqs, heads, _, local_len, _ = fv.shape
    width = weight.shape[1]
    group = 4
    return pl.pallas_call(
        output_kernel,
        grid=(seqs // group,),
        in_specs=[
            vmem_spec(),
            pl.BlockSpec((3, group // 2, heads, PAIR, HK), lambda i: (0, i, 0, 0, 0)),
            pl.BlockSpec((group, heads, 1, local_len, HK), lambda i: (i, 0, 1, 0, 0)),
            vmem_spec(),
            vmem_spec(),
            vmem_spec(),
        ],
        out_specs=pl.BlockSpec((group, local_len, width), lambda i: (i, 0, 0)),
        out_shape=jax.ShapeDtypeStruct((seqs, local_len, width), BF16),
        compiler_params=limit(12),
        name="output",
    )(states, parts, fv, weight, norm_gain.reshape(1, HV), post_gain.reshape(1, width))


def layer(
    tokens,
    pre_gain,
    w_query,
    w_forget,
    w_value,
    w_gate,
    lower_bound,
    extra_decay,
    initial_state,
    norm_gain,
    w_out,
    post_gain,
):
    seqs, local_len, width = tokens.shape
    items = seqs * HEADS
    wide = HEADS * HV
    where = jnp.stack([lax.axis_index("y"), lax.axis_index("c")]).astype(jnp.int32)
    gaps = (1.0 - lower_bound).reshape(HEADS, HK)

    first = jnp.concatenate([w_forget, w_value], axis=1)
    stacked = [w_out[:, n * wide : (n + 1) * wide] for n in range(width // wide)]
    second = jnp.concatenate([w_query, w_gate, jnp.concatenate(stacked, axis=0)], axis=1)
    gap = lax.dynamic_slice_in_dim(gaps, lax.axis_index("x"), 1, 0)
    run = jnp.cumsum(extra_decay.reshape(items, CHUNK), axis=1)
    high = lax.reduce_precision(run, 8, 7)
    middle = lax.reduce_precision(run - high, 8, 7)
    low = run - high - middle
    tail = jnp.stack([high, middle, low] + [jnp.zeros_like(high)] * (TAIL - 3), axis=1)
    tail = jnp.concatenate([tail, tail], axis=2).astype(BF16)
    run = run.reshape(items // 2, PAIR)
    state = initial_state[0].T
    normed = normed_tokens(tokens.reshape(seqs * local_len, width), pre_gain, where)

    early = (second, gap, run, tail, state, normed)
    first_own = gathered_y(first, ((), (), early, ()))
    first_other = swapped(first_own)
    fv = project_heads(normed, first_own, first_other, seqs, local_len)
    moved = lax.all_to_all(fv.reshape(items, 2 * local_len, HK), SP, 0, 0, tiled=True)
    starts = chunk_states(moved.reshape(items, 2, local_len, HK), run, tail, gap, state)
    states = lax.all_to_all(starts, SP, 0, 0, tiled=True)

    second_own = gathered_y(second, ((first_own,), (fv,), (), (starts,)))
    second_other = swapped(second_own)
    parts = local_parts(normed, second_own, second_other, fv, gaps)
    weight = out_weight(where, second_own, second_other, width)
    states = states.reshape(seqs, HEADS, HV + TAIL, HK)
    return output_rows(states, parts, fv, weight, norm_gain, post_gain)


def solution(mesh):
    split = Mesh(mesh.devices.reshape(8, 4, 8, 2), ("z", "x", "y", "c"))
    in_specs = (
        P(DP, SP, None),
        P(),
        P(DP, None),
        P(DP, None),
        P(DP, None),
        P(DP, None),
        P(),
        P(DP_SP, None),
        P(DP_SP, None, None),
        P(),
        P(DP, None),
        P(),
    )
    out_specs = P(DP, SP, None)
    return jax.shard_map(layer, mesh=split, in_specs=in_specs, out_specs=out_specs, check_vma=False)
```

profile of v0, /device:TPU:1, one launch (start us, length us, event | category | flops | bytes accessed | tf_op | source)
XLA Modules:
  0.0 183.9 jit_solution(13238253563696154149)
XLA Ops:
  1.8 5.9 %collective-permute-start.1 = (bf16[128,1024]{1,0:T(8,128)(2,1)S(1)}, bf16[128,1024]{1,0:T(8,128)(2,1)S(1)}, u32[]{:S(2)}, u32[]{:S(2)}) collective-permute-start(bf16[128,1024]{1,0:T(8,128)(2,1)S(1)} %constant_dynamic-update-slice_fusion.refs_0_), channel_id=1, source_target_pairs={{0,14},{2,0},{4,2},{6,4},{8,6},{10,8},{12,10},{14,12},{1,15},{3,1}... | collective-permute-start | bytes 786440 | tf_op jit(solution)/shard_map/ppermute | solution.py:31
  7.8 1.9 %collective-permute-start = (bf16[128,1024]{1,0:T(8,128)(2,1)S(1)}, bf16[128,1024]{1,0:T(8,128)(2,1)S(1)}, u32[]{:S(2)}, u32[]{:S(2)}) collective-permute-start(bf16[128,1024]{1,0:T(8,128)(2,1)S(1)} %constant_dynamic-update-slice_fusion.refs_0_), channel_id=1, source_target_pairs={{0,2},{2,4},{4,6},{6,8},{8,10},{10,12},{12,14},{14,0},{1,3},{3,5},... | collective-permute-start | bytes 786440 | tf_op jit(solution)/shard_map/ppermute | solution.py:31
  13.8 4.6 %collective-permute-start.3 = (bf16[128,1024]{1,0:T(8,128)(2,1)S(1)}, bf16[128,1024]{1,0:T(8,128)(2,1)S(1)}, u32[]{:S(2)}, u32[]{:S(2)}) collective-permute-start(bf16[128,1024]{1,0:T(8,128)(2,1)S(1)} %collective-permute-done.1.refs_2_), channel_id=1, source_target_pairs={{0,14},{2,0},{4,2},{6,4},{8,6},{10,8},{12,10},{14,12},{1,15},{3,1}... | collective-permute-start | bytes 786440 | tf_op jit(solution)/shard_map/ppermute | solution.py:31
  28.6 4.6 %collective-permute-start.5 = (bf16[128,1024]{1,0:T(8,128)(2,1)S(1)}, bf16[128,1024]{1,0:T(8,128)(2,1)S(1)}, u32[]{:S(2)}, u32[]{:S(2)}) collective-permute-start(bf16[128,1024]{1,0:T(8,128)(2,1)S(1)} %collective-permute-done.3.refs_4_), channel_id=1, source_target_pairs={{0,14},{2,0},{4,2},{6,4},{8,6},{10,8},{12,10},{14,12},{1,15},{3,1}... | collective-permute-start | bytes 786440 | tf_op jit(solution)/shard_map/ppermute | solution.py:31
  37.0 4.6 %collective-permute-start.7 = (bf16[64,1024]{1,0:T(8,128)(2,1)S(1)}, bf16[64,1024]{1,0:T(8,128)(2,1)S(1)}, u32[]{:S(2)}, u32[]{:S(2)}) collective-permute-start(bf16[64,1024]{1,0:T(8,128)(2,1)S(1)} %slice.33), channel_id=1, source_target_pairs={{0,14},{2,0},{4,2},{6,4},{8,6},{10,8},{12,10},{14,12},{1,15},{3,1}... | collective-permute-start | bytes 393224 | tf_op jit(solution)/shard_map/ppermute | solution.py:31
  43.6 8.7 %collective-permute-start.8 = (bf16[1024,1024]{1,0:T(8,128)(2,1)S(1)}, bf16[1024,1024]{1,0:T(8,128)(2,1)S(1)}, u32[]{:S(2)}, u32[]{:S(2)}) collective-permute-start(bf16[1024,1024]{1,0:T(8,128)(2,1)S(1)} %stack.25.own_ref), channel_id=1, source_target_pairs={{0,1},{1,0},{2,3},{3,2},{4,5},{5,4},{6,7},{7,6},{8,9},{9,8},{10,11... | collective-permute-start | bytes 6291464 | tf_op jit(solution)/shard_map/ppermute | solution.py:35
  52.4 3.8 %collective-permute-done.8.other_ref = bf16[1024,1024]{1,0:T(8,128)(2,1)S(1)} collective-permute-done((bf16[1024,1024]{1,0:T(8,128)(2,1)S(1)}, bf16[1024,1024]{1,0:T(8,128)(2,1)S(1)}, u32[]{:S(2)}, u32[]{:S(2)}) %collective-permute-start.8) | collective-permute-done | bytes 2097184 | tf_op jit(solution)/shard_map/ppermute | solution.py:35
  56.1 3.8 %project.1.fv_ref = bf16[8,4,2,64,128]{4,3,2,1,0:T(8,128)(2,1)} custom-call(bf16[512,2048]{1,0:T(8,128)(2,1)S(1)} %norm.1.a_ref, bf16[1024,1024]{1,0:T(8,128)(2,1)S(1)} %stack.25.own_ref, bf16[1024,1024]{1,0:T(8,128)(2,1)S(1)} %collective-permute-done.8.other_ref), custom_call_target="tpu_custom_call" | custom-call | tf_op jit(solution)/shard_map/project/pallas_call | solution.py:149
  59.9 11.8 %all-to-all-start = ((bf16[32,128,128]{2,1,0:T(8,128)(2,1)}), bf16[32,128,128]{2,1,0:T(8,128)(2,1)S(1)}, u32[]{:S(2)}, u32[]{:S(2)}) async-start(bf16[32,128,128]{2,1,0:T(8,128)(2,1)} %bitcast.15), calls=%async_computation | async-start | bytes 2097152 | tf_op jit(solution)/shard_map/all_to_all | solution.py:378
  73.7 5.3 %collective-permute-start.10 = (bf16[128,1536]{1,0:T(8,128)(2,1)S(1)}, bf16[128,1536]{1,0:T(8,128)(2,1)S(1)}, u32[]{:S(2)}, u32[]{:S(2)}) collective-permute-start(bf16[128,1536]{1,0:T(8,128)(2,1)S(1)} %maximum_maximum_fusion.refs_0_), channel_id=1, source_target_pairs={{0,14},{2,0},{4,2},{6,4},{8,6},{10,8},{12,10},{14,12},{1,15},{3,1}... | collective-permute-start | bytes 1179656 | tf_op jit(solution)/shard_map/ppermute | solution.py:31
  79.0 6.9 %collective-permute-done.9.refs_1_ = bf16[128,1536]{1,0:T(8,128)(2,1)S(1)} collective-permute-done((bf16[128,1536]{1,0:T(8,128)(2,1)S(1)}, bf16[128,1536]{1,0:T(8,128)(2,1)S(1)}, u32[]{:S(2)}, u32[]{:S(2)}) %collective-permute-start.9) | collective-permute-done | bytes 393248 | tf_op jit(solution)/shard_map/ppermute | solution.py:31
  86.8 3.3 %collective-permute-start.11 = (bf16[128,1536]{1,0:T(8,128)(2,1)S(1)}, bf16[128,1536]{1,0:T(8,128)(2,1)S(1)}, u32[]{:S(2)}, u32[]{:S(2)}) collective-permute-start(bf16[128,1536]{1,0:T(8,128)(2,1)S(1)} %collective-permute-done.9.refs_1_), channel_id=1, source_target_pairs={{0,2},{2,4},{4,6},{6,8},{8,10},{10,12},{12,14},{14,0},{1,3},{3,5},... | collective-permute-start | bytes 1179656 | tf_op jit(solution)/shard_map/ppermute | solution.py:31
  90.8 3.9 %collective-permute-start.12 = (bf16[128,1536]{1,0:T(8,128)(2,1)S(1)}, bf16[128,1536]{1,0:T(8,128)(2,1)S(1)}, u32[]{:S(2)}, u32[]{:S(2)}) collective-permute-start(bf16[128,1536]{1,0:T(8,128)(2,1)S(1)} %collective-permute-done.10.refs_2_), channel_id=1, source_target_pairs={{0,14},{2,0},{4,2},{6,4},{8,6},{10,8},{12,10},{14,12},{1,15},{3,1}... | collective-permute-start | bytes 1179656 | tf_op jit(solution)/shard_map/ppermute | solution.py:31
  95.5 4.6 %collective-permute-done.11.refs_3_ = bf16[128,1536]{1,0:T(8,128)(2,1)S(1)} collective-permute-done((bf16[128,1536]{1,0:T(8,128)(2,1)S(1)}, bf16[128,1536]{1,0:T(8,128)(2,1)S(1)}, u32[]{:S(2)}, u32[]{:S(2)}) %collective-permute-start.11) | collective-permute-done | bytes 393248 | tf_op jit(solution)/shard_map/ppermute | solution.py:31
  102.0 5.0 %collective-permute-start.14 = (bf16[128,1536]{1,0:T(8,128)(2,1)S(1)}, bf16[128,1536]{1,0:T(8,128)(2,1)S(1)}, u32[]{:S(2)}, u32[]{:S(2)}) collective-permute-start(bf16[128,1536]{1,0:T(8,128)(2,1)S(1)} %collective-permute-done.12.refs_4_), channel_id=1, source_target_pairs={{0,14},{2,0},{4,2},{6,4},{8,6},{10,8},{12,10},{14,12},{1,15},{3,1}... | collective-permute-start | bytes 1179656 | tf_op jit(solution)/shard_map/ppermute | solution.py:31
  107.0 3.3 %state.1 = bf16[32,136,128]{2,1,0:T(8,128)(2,1)} custom-call(bf16[32,2,64,128]{3,2,1,0:T(8,128)(2,1)S(1)} %bitcast.16, f32[16,128]{1,0:T(8,128)S(1)} %reshape.58.run_ref, bf16[32,8,128]{2,1,0:T(8,128)(2,1)S(1)} %pad_maximum_fusion.tail_ref, f32[1,128]{1,0:T(1,128)S(1)} %constant_dynamic-slice_fusion.gap_ref, f32[128,128]{1,0:T(8,128)S(1)} %bitcast.18), custom_call_target="tpu_custom_call" | custom-call | tf_op jit(solution)/shard_map/state/pallas_call | solution.py:210
  113.1 5.3 %collective-permute-start.16 = (bf16[64,1536]{1,0:T(8,128)(2,1)S(1)}, bf16[64,1536]{1,0:T(8,128)(2,1)S(1)}, u32[]{:S(2)}, u32[]{:S(2)}) collective-permute-start(bf16[64,1536]{1,0:T(8,128)(2,1)S(1)} %slice.31), channel_id=1, source_target_pairs={{0,14},{2,0},{4,2},{6,4},{8,6},{10,8},{12,10},{14,12},{1,15},{3,1}... | collective-permute-start | bytes 589832 | tf_op jit(solution)/shard_map/ppermute | solution.py:31
  121.1 5.0 %collective-permute-done.15.refs_7_ = bf16[64,1536]{1,0:T(8,128)(2,1)S(1)} collective-permute-done((bf16[64,1536]{1,0:T(8,128)(2,1)S(1)}, bf16[64,1536]{1,0:T(8,128)(2,1)S(1)}, u32[]{:S(2)}, u32[]{:S(2)}) %collective-permute-start.15) | collective-permute-done | bytes 196640 | tf_op jit(solution)/shard_map/ppermute | solution.py:31
  130.3 6.6 %collective-permute-start.17 = (bf16[1024,1536]{1,0:T(8,128)(2,1)S(1)}, bf16[1024,1536]{1,0:T(8,128)(2,1)}, u32[]{:S(2)}, u32[]{:S(2)}) collective-permute-start(bf16[1024,1536]{1,0:T(8,128)(2,1)S(1)} %stack.26.own_ref), channel_id=1, source_target_pairs={{0,1},{1,0},{2,3},{3,2},{4,5},{5,4},{6,7},{7,6},{8,9},{9,8},{10,11... | collective-permute-start | bytes 9437192 | tf_op jit(solution)/shard_map/ppermute | solution.py:35
  136.8 8.8 %all-to-all-start.1 = ((bf16[32,136,128]{2,1,0:T(8,128)(2,1)}), bf16[32,136,128]{2,1,0:T(8,128)(2,1)}, u32[]{:S(2)}, u32[]{:S(2)}) async-start(bf16[32,136,128]{2,1,0:T(8,128)(2,1)} %state.1), calls=%async_computation.1 | async-start | bytes 2228224 | tf_op jit(solution)/shard_map/all_to_all | solution.py:380
  148.5 6.6 %local.1.part_ref = bf16[3,4,4,128,128]{4,3,2,1,0:T(8,128)(2,1)} custom-call(bf16[512,2048]{1,0:T(8,128)(2,1)S(1)} %copy-done.1, bf16[1024,1536]{1,0:T(8,128)(2,1)S(1)} %stack.26.own_ref, bf16[1024,1536]{1,0:T(8,128)(2,1)} %collective-permute-done.17.other_ref, bf16[8,4,2,64,128]{4,3,2,1,0:T(8,128)(2,1)S(1)} %copy-done.2, ...), custom_call_target="tpu_custom_call" | custom-call | tf_op jit(solution)/shard_map/local/pallas_call | solution.py:265
  155.1 2.1 %weight.1.weight_ref = bf16[512,2048]{1,0:T(8,128)(2,1)S(1)} custom-call(s32[2]{0:T(128)S(1)} %pad_add_fusion.where_ref, bf16[1024,1536]{1,0:T(8,128)(2,1)S(1)} %stack.26.own_ref, bf16[1024,1536]{1,0:T(8,128)(2,1)} %collective-permute-done.17.other_ref), custom_call_target="tpu_custom_call" | custom-call | tf_op jit(solution)/shard_map/weight/pallas_call | solution.py:275
  158.5 15.8 %all-to-all-done.1 = bf16[32,136,128]{2,1,0:T(8,128)(2,1)} async-done(((bf16[32,136,128]{2,1,0:T(8,128)(2,1)}), bf16[32,136,128]{2,1,0:T(8,128)(2,1)}, u32[]{:S(2)}, u32[]{:S(2)}) %all-to-all-start.1) | async-done | bytes 1114144 | tf_op jit(solution)/shard_map/all_to_all | solution.py:380
  178.5 5.4 %output.1 = bf16[8,64,2048]{2,1,0:T(8,128)(2,1)} custom-call(bf16[8,4,136,128]{3,2,1,0:T(8,128)(2,1)} %bitcast.10.state_ref, bf16[3,4,4,128,128]{4,3,2,1,0:T(8,128)(2,1)S(1)} %copy-done.6, bf16[8,4,2,64,128]{4,3,2,1,0:T(8,128)(2,1)S(1)} %copy-done.3, bf16[512,2048]{1,0:T(8,128)(2,1)S(1)} %copy-done.5, f32[1,128]{1,0:T(1,128)S(1)} %bitcast.21, ...), custom_call_target="tpu_custom_call" | custom-call | tf_op jit(solution)/shard_map/output/pallas_call | solution.py:322
  (96 shorter events, 45.9 us)
Async XLA Ops:
  1.8 11.9 %collective-permute-start.1 = (bf16[128,1024]{1,0:T(8,128)(2,1)S(1)}, bf16[128,1024]{1,0:T(8,128)(2,1)S(1)}, u32[]{:S(2)}, u32[]{:S(2)}) collective-permute-start(bf16[128,1024]{1,0:T(8,128)(2,1)S(1)} %constant_dynamic-update-slice_fusion.refs_0_), channel_id=1, source_target_pairs={{0,14},{2,0},{4,2},{6,4},{8,6},{10,8},{12,10},{14,12},{1,15},{3,1}... | collective-permute-start | bytes 786440 | tf_op jit(solution)/shard_map/ppermute | solution.py:31
  7.8 10.6 %collective-permute-start = (bf16[128,1024]{1,0:T(8,128)(2,1)S(1)}, bf16[128,1024]{1,0:T(8,128)(2,1)S(1)}, u32[]{:S(2)}, u32[]{:S(2)}) collective-permute-start(bf16[128,1024]{1,0:T(8,128)(2,1)S(1)} %constant_dynamic-update-slice_fusion.refs_0_), channel_id=1, source_target_pairs={{0,2},{2,4},{4,6},{6,8},{8,10},{10,12},{12,14},{14,0},{1,3},{3,5},... | collective-permute-start | bytes 786440 | tf_op jit(solution)/shard_map/ppermute | solution.py:31
  13.8 11.7 %collective-permute-start.3 = (bf16[128,1024]{1,0:T(8,128)(2,1)S(1)}, bf16[128,1024]{1,0:T(8,128)(2,1)S(1)}, u32[]{:S(2)}, u32[]{:S(2)}) collective-permute-start(bf16[128,1024]{1,0:T(8,128)(2,1)S(1)} %collective-permute-done.1.refs_2_), channel_id=1, source_target_pairs={{0,14},{2,0},{4,2},{6,4},{8,6},{10,8},{12,10},{14,12},{1,15},{3,1}... | collective-permute-start | bytes 786440 | tf_op jit(solution)/shard_map/ppermute | solution.py:31
  18.3 8.3 %collective-permute-start.2 = (bf16[128,1024]{1,0:T(8,128)(2,1)S(1)}, bf16[128,1024]{1,0:T(8,128)(2,1)S(1)}, u32[]{:S(2)}, u32[]{:S(2)}) collective-permute-start(bf16[128,1024]{1,0:T(8,128)(2,1)S(1)} %collective-permute-done.refs_1_), channel_id=1, source_target_pairs={{0,2},{2,4},{4,6},{6,8},{8,10},{10,12},{12,14},{14,0},{1,3},{3,5},... | collective-permute-start | bytes 786440 | tf_op jit(solution)/shard_map/ppermute | solution.py:31
  25.4 30.8 %copy-start = (bf16[512,2048]{1,0:T(8,128)(2,1)}, bf16[512,2048]{1,0:T(8,128)(2,1)S(1)}, u32[]{:S(2)}) copy-start(bf16[512,2048]{1,0:T(8,128)(2,1)S(1)} %norm.1.a_ref) | copy-start | bytes 6291460
  26.7 8.3 %collective-permute-start.4 = (bf16[128,1024]{1,0:T(8,128)(2,1)S(1)}, bf16[128,1024]{1,0:T(8,128)(2,1)S(1)}, u32[]{:S(2)}, u32[]{:S(2)}) collective-permute-start(bf16[128,1024]{1,0:T(8,128)(2,1)S(1)} %collective-permute-done.2.refs_3_), channel_id=1, source_target_pairs={{0,2},{2,4},{4,6},{6,8},{8,10},{10,12},{12,14},{14,0},{1,3},{3,5},... | collective-permute-start | bytes 786440 | tf_op jit(solution)/shard_map/ppermute | solution.py:31
  28.6 8.3 %collective-permute-start.5 = (bf16[128,1024]{1,0:T(8,128)(2,1)S(1)}, bf16[128,1024]{1,0:T(8,128)(2,1)S(1)}, u32[]{:S(2)}, u32[]{:S(2)}) collective-permute-start(bf16[128,1024]{1,0:T(8,128)(2,1)S(1)} %collective-permute-done.3.refs_4_), channel_id=1, source_target_pairs={{0,14},{2,0},{4,2},{6,4},{8,6},{10,8},{12,10},{14,12},{1,15},{3,1}... | collective-permute-start | bytes 786440 | tf_op jit(solution)/shard_map/ppermute | solution.py:31
  35.0 6.9 %collective-permute-start.6 = (bf16[64,1024]{1,0:T(8,128)(2,1)S(1)}, bf16[64,1024]{1,0:T(8,128)(2,1)S(1)}, u32[]{:S(2)}, u32[]{:S(2)}) collective-permute-start(bf16[64,1024]{1,0:T(8,128)(2,1)S(1)} %slice.32), channel_id=1, source_target_pairs={{0,2},{2,4},{4,6},{6,8},{8,10},{10,12},{12,14},{14,0},{1,3},{3,5},... | collective-permute-start | bytes 393224 | tf_op jit(solution)/shard_map/ppermute | solution.py:31
  37.0 6.5 %collective-permute-start.7 = (bf16[64,1024]{1,0:T(8,128)(2,1)S(1)}, bf16[64,1024]{1,0:T(8,128)(2,1)S(1)}, u32[]{:S(2)}, u32[]{:S(2)}) collective-permute-start(bf16[64,1024]{1,0:T(8,128)(2,1)S(1)} %slice.33), channel_id=1, source_target_pairs={{0,14},{2,0},{4,2},{6,4},{8,6},{10,8},{12,10},{14,12},{1,15},{3,1}... | collective-permute-start | bytes 393224 | tf_op jit(solution)/shard_map/ppermute | solution.py:31
  43.6 12.5 %collective-permute-start.8 = (bf16[1024,1024]{1,0:T(8,128)(2,1)S(1)}, bf16[1024,1024]{1,0:T(8,128)(2,1)S(1)}, u32[]{:S(2)}, u32[]{:S(2)}) collective-permute-start(bf16[1024,1024]{1,0:T(8,128)(2,1)S(1)} %stack.25.own_ref), channel_id=1, source_target_pairs={{0,1},{1,0},{2,3},{3,2},{4,5},{5,4},{6,7},{7,6},{8,9},{9,8},{10,11... | collective-permute-start | bytes 6291464 | tf_op jit(solution)/shard_map/ppermute | solution.py:35
  59.9 47.1 %all-to-all-start = ((bf16[32,128,128]{2,1,0:T(8,128)(2,1)}), bf16[32,128,128]{2,1,0:T(8,128)(2,1)S(1)}, u32[]{:S(2)}, u32[]{:S(2)}) async-start(bf16[32,128,128]{2,1,0:T(8,128)(2,1)} %bitcast.15), calls=%async_computation | async-start | bytes 2097152 | tf_op jit(solution)/shard_map/all_to_all | solution.py:378
  71.7 14.1 %collective-permute-start.9 = (bf16[128,1536]{1,0:T(8,128)(2,1)S(1)}, bf16[128,1536]{1,0:T(8,128)(2,1)S(1)}, u32[]{:S(2)}, u32[]{:S(2)}) collective-permute-start(bf16[128,1536]{1,0:T(8,128)(2,1)S(1)} %maximum_maximum_fusion.refs_0_), channel_id=1, source_target_pairs={{0,2},{2,4},{4,6},{6,8},{8,10},{10,12},{12,14},{14,0},{1,3},{3,5},... | collective-permute-start | bytes 1179656 | tf_op jit(solution)/shard_map/ppermute | solution.py:31
  73.7 13.1 %collective-permute-start.10 = (bf16[128,1536]{1,0:T(8,128)(2,1)S(1)}, bf16[128,1536]{1,0:T(8,128)(2,1)S(1)}, u32[]{:S(2)}, u32[]{:S(2)}) collective-permute-start(bf16[128,1536]{1,0:T(8,128)(2,1)S(1)} %maximum_maximum_fusion.refs_0_), channel_id=1, source_target_pairs={{0,14},{2,0},{4,2},{6,4},{8,6},{10,8},{12,10},{14,12},{1,15},{3,1}... | collective-permute-start | bytes 1179656 | tf_op jit(solution)/shard_map/ppermute | solution.py:31
  86.8 13.3 %collective-permute-start.11 = (bf16[128,1536]{1,0:T(8,128)(2,1)S(1)}, bf16[128,1536]{1,0:T(8,128)(2,1)S(1)}, u32[]{:S(2)}, u32[]{:S(2)}) collective-permute-start(bf16[128,1536]{1,0:T(8,128)(2,1)S(1)} %collective-permute-done.9.refs_1_), channel_id=1, source_target_pairs={{0,2},{2,4},{4,6},{6,8},{8,10},{10,12},{12,14},{14,0},{1,3},{3,5},... | collective-permute-start | bytes 1179656 | tf_op jit(solution)/shard_map/ppermute | solution.py:31
  90.8 11.1 %collective-permute-start.12 = (bf16[128,1536]{1,0:T(8,128)(2,1)S(1)}, bf16[128,1536]{1,0:T(8,128)(2,1)S(1)}, u32[]{:S(2)}, u32[]{:S(2)}) collective-permute-start(bf16[128,1536]{1,0:T(8,128)(2,1)S(1)} %collective-permute-done.10.refs_2_), channel_id=1, source_target_pairs={{0,14},{2,0},{4,2},{6,4},{8,6},{10,8},{12,10},{14,12},{1,15},{3,1}... | collective-permute-start | bytes 1179656 | tf_op jit(solution)/shard_map/ppermute | solution.py:31
  100.1 21.0 %copy-start.16 = (bf16[128,1536]{1,0:T(8,128)(2,1)}, bf16[128,1536]{1,0:T(8,128)(2,1)S(1)}, u32[]{:S(2)}) copy-start(bf16[128,1536]{1,0:T(8,128)(2,1)S(1)} %collective-permute-done.11.refs_3_) | copy-start | bytes 1179652
  100.1 11.7 %collective-permute-start.13 = (bf16[128,1536]{1,0:T(8,128)(2,1)S(1)}, bf16[128,1536]{1,0:T(8,128)(2,1)S(1)}, u32[]{:S(2)}, u32[]{:S(2)}) collective-permute-start(bf16[128,1536]{1,0:T(8,128)(2,1)S(1)} %collective-permute-done.11.refs_3_), channel_id=1, source_target_pairs={{0,2},{2,4},{4,6},{6,8},{8,10},{10,12},{12,14},{14,0},{1,3},{3,5},... | collective-permute-start | bytes 1179656 | tf_op jit(solution)/shard_map/ppermute | solution.py:31
  102.0 11.1 %collective-permute-start.14 = (bf16[128,1536]{1,0:T(8,128)(2,1)S(1)}, bf16[128,1536]{1,0:T(8,128)(2,1)S(1)}, u32[]{:S(2)}, u32[]{:S(2)}) collective-permute-start(bf16[128,1536]{1,0:T(8,128)(2,1)S(1)} %collective-permute-done.12.refs_4_), channel_id=1, source_target_pairs={{0,14},{2,0},{4,2},{6,4},{8,6},{10,8},{12,10},{14,12},{1,15},{3,1}... | collective-permute-start | bytes 1179656 | tf_op jit(solution)/shard_map/ppermute | solution.py:31
  113.1 7.9 %collective-permute-start.16 = (bf16[64,1536]{1,0:T(8,128)(2,1)S(1)}, bf16[64,1536]{1,0:T(8,128)(2,1)S(1)}, u32[]{:S(2)}, u32[]{:S(2)}) collective-permute-start(bf16[64,1536]{1,0:T(8,128)(2,1)S(1)} %slice.31), channel_id=1, source_target_pairs={{0,14},{2,0},{4,2},{6,4},{8,6},{10,8},{12,10},{14,12},{1,15},{3,1}... | collective-permute-start | bytes 589832 | tf_op jit(solution)/shard_map/ppermute | solution.py:31
  118.5 7.6 %collective-permute-start.15 = (bf16[64,1536]{1,0:T(8,128)(2,1)S(1)}, bf16[64,1536]{1,0:T(8,128)(2,1)S(1)}, u32[]{:S(2)}, u32[]{:S(2)}) collective-permute-start(bf16[64,1536]{1,0:T(8,128)(2,1)S(1)} %slice.30), channel_id=1, source_target_pairs={{0,2},{2,4},{4,6},{6,8},{8,10},{10,12},{12,14},{14,0},{1,3},{3,5},... | collective-permute-start | bytes 589832 | tf_op jit(solution)/shard_map/ppermute | solution.py:31
  130.3 15.4 %collective-permute-start.17 = (bf16[1024,1536]{1,0:T(8,128)(2,1)S(1)}, bf16[1024,1536]{1,0:T(8,128)(2,1)}, u32[]{:S(2)}, u32[]{:S(2)}) collective-permute-start(bf16[1024,1536]{1,0:T(8,128)(2,1)S(1)} %stack.26.own_ref), channel_id=1, source_target_pairs={{0,1},{1,0},{2,3},{3,2},{4,5},{5,4},{6,7},{7,6},{8,9},{9,8},{10,11... | collective-permute-start | bytes 9437192 | tf_op jit(solution)/shard_map/ppermute | solution.py:35
  136.8 37.4 %all-to-all-start.1 = ((bf16[32,136,128]{2,1,0:T(8,128)(2,1)}), bf16[32,136,128]{2,1,0:T(8,128)(2,1)}, u32[]{:S(2)}, u32[]{:S(2)}) async-start(bf16[32,136,128]{2,1,0:T(8,128)(2,1)} %state.1), calls=%async_computation.1 | async-start | bytes 2228224 | tf_op jit(solution)/shard_map/all_to_all | solution.py:380
  155.1 19.2 %copy-start.21 = (f32[2048]{0:T(1024)S(1)}, f32[2048]{0:T(1024)}, u32[]{:S(2)}) copy-start(f32[2048]{0:T(1024)} %param.23) | copy-start | bytes 24580
  155.1 19.2 %copy-start.22 = (f32[128]{0:T(128)S(1)}, f32[128]{0:T(128)}, u32[]{:S(2)}) copy-start(f32[128]{0:T(128)} %param.21) | copy-start | bytes 1540
  (21 other events, 94.2 us)
where the time goes:
time: 186 us; the launch traced here: 184 us
  starting transfers between devices  91.8 us (49%)
  waiting for transfers between devices  45.3 us (24%)
  Pallas kernels  23.3 us (13%)
  local copies, waits for them, and re-layouts  20.6 us (11%)
  other arithmetic  2.48 us (1%)
    ppermute x16, starting transfers between devices, shifted(): return lax.ppermute(a, 'y', [(i, (i + step) % size) for i in range(size)])  55.9 us
    ppermute x16, waiting for transfers between devices, shifted(): return lax.ppermute(a, 'y', [(i, (i + step) % size) for i in range(size)])  25.7 us
    unnamed x53, local copies, waits for them, and re-layouts  18.5 us
    all_to_all x1, waiting for transfers between devices, layer(): states = lax.all_to_all(starts, SP, 0, 0, tiled=True)  15.8 us
    ppermute x2, starting transfers between devices, swapped(): return lax.ppermute(a, 'c', [(0, 1), (1, 0)])  15.3 us
    all_to_all x1, starting transfers between devices, layer(): lax.all_to_all(fv.reshape(items, 2 * local_len, HK), SP, 0, 0, tiled=True)  11.8 us
    all_to_all x1, starting transfers between devices, layer(): states = lax.all_to_all(starts, SP, 0, 0, tiled=True)  8.78 us
    pallas_call x1, Pallas kernels, local_parts(): pl.pallas_call(local_kernel, in_specs=[vmem_spec()] * 5, out_shape=pltpu....  6.62 us
  transfers between devices with their start and end apart: 20, of which 13 were waited for; matrix products, arithmetic and copies ran while one was open for 3% of the time, Pallas kernels for 7%

commit v1 on v0

--- a/solution.py
+++ b/solution.py
@@ -1,3 +1,5 @@
+import functools
+
 import jax
 import jax.numpy as jnp
 from jax import lax
@@ -20,6 +22,7 @@
 ROWS = 128
 OUT_ROWS = 32
 EPS = 1e-06
+WIDE = HEADS * HV
 
 
 F32 = jnp.float32
@@ -41,16 +44,48 @@
 
 def gathered_y(shard, waits):
     pieces = [shard]
+    own, other = [], []
     up = down = shard
-    for k in range(3):
+    for k in range(4):
         up, down = after((up, down), waits[k]) if waits[k] else (up, down)
-        up, down = shifted(up, 1), shifted(down, -1)
-        pieces += [up, down]
-    up, down = after((up, down), waits[3]) if waits[3] else (up, down)
-    half = shard.shape[0] // 2
-    up, down = up[:half], down[half:]
-    pieces += [shifted(up, 1), shifted(down, -1)]
-    return stacked_pieces(pieces)
+        up = shifted(up, 1)
+        down = shifted(down, -1) if k < 3 else None
+        if k in (2, 3):
+            own.append(stacked_pieces(pieces) if len(pieces) > 1 else pieces[0])
+            other.append(swapped(own[-1]))
+            pieces = []
+        pieces += [up, down] if k < 3 else [up]
+    own.append(pieces[0])
+    other.append(swapped(pieces[0]))
+    return own, other
+
+
+def in_hbm(a):
+    return pltpu.with_memory_space_constraint(a, pltpu.HBM)
+
+
+def join_kernel(*refs, places):
+    out_ref, sems = refs[-2:]
+    copies = []
+    for n, (k, (rows, cols), (r, c)) in enumerate(places):
+        source = refs[k].at[:, pl.ds(cols, WIDE)]
+        target = out_ref.at[pl.ds(r, source.shape[0]), pl.ds(c, WIDE)]
+        copies.append(pltpu.make_async_copy(source, target, sems.at[n]))
+    for copy in copies:
+        copy.start()
+    for copy in copies:
+        copy.wait()
+
+
+def joined(arrays, places, width):
+    return pl.pallas_call(
+        functools.partial(join_kernel, places=places),
+        in_specs=[pl.BlockSpec(memory_space=pl.ANY)] * len(arrays),
+        out_specs=vmem_spec(),
+        out_shape=jax.ShapeDtypeStruct((ROWS, width), BF16),
+        scratch_shapes=[pltpu.SemaphoreType.DMA((len(places),))],
+        compiler_params=limit(2),
+    )(*[in_hbm(a) for a in arrays])
 
 
 def stack_kernel(*refs):
@@ -69,9 +104,20 @@
         in_specs=[vmem_spec()] * len(pieces),
         out_specs=vmem_spec(),
         out_shape=jax.ShapeDtypeStruct((rows, pieces[0].shape[1]), BF16),
-        compiler_params=limit(8),
+        compiler_params=limit(6),
         name="stack",
     )(*pieces)
+
+
+def against(a_ref, refs, cols):
+    total = None
+    first = 0
+    for ref in refs:
+        rows = ref.shape[0]
+        part = dot(a_ref[:, first : first + rows], ref[:, cols])
+        total = part if total is None else total + part
+        first += rows
+    return total
 
 
 def dot(a, b):
@@ -122,7 +168,7 @@
         out_shape=jax.ShapeDtypeStruct((rows, width), BF16),
         compiler_params=pltpu.CompilerParams(vmem_limit_bytes=6 << 20),
         name="norm",
-    )(where, tokens, pre_gain.reshape(1, width))
+    )(where, in_hbm(tokens), pre_gain.reshape(1, width))
 
 
 def vmem_spec():
@@ -133,28 +179,27 @@
     return pltpu.CompilerParams(vmem_limit_bytes=mib << 20)
 
 
-def project_kernel(a_ref, own_ref, other_ref, out_ref):
-    half = own_ref.shape[0]
+def project_kernel(a_ref, *refs):
+    out_ref = refs[-1]
     seqs, heads, _, local_len, _ = out_ref.shape
     wide = heads * HK
     cols = pl.ds(pl.multiple_of(pl.program_id(0) * wide, wide), wide)
-    total = dot(a_ref[:, :half], own_ref[:, cols]) + dot(a_ref[:, half:], other_ref[:, cols])
-    total = total.astype(BF16)
+    total = against(a_ref, refs[:-1], cols).astype(BF16)
     for n in range(heads):
         out_ref[:, n, 0] = total[:, n * HK : (n + 1) * HK].reshape(seqs, local_len, HK)
 
 
-def project_heads(normed, own, other, seqs, local_len):
+def project_heads(normed, stacks, seqs, local_len):
     block = (seqs, 2, 1, local_len, HK)
     return pl.pallas_call(
         project_kernel,
         grid=(HEADS,),
-        in_specs=[vmem_spec()] * 3,
+        in_specs=[vmem_spec()] * (1 + len(stacks)),
         out_specs=pl.BlockSpec(block, lambda j: (0, j % 2, j // 2, 0, 0)),
         out_shape=pltpu.HBM((seqs, HEADS, 2, local_len, HK), BF16),
         compiler_params=limit(8),
         name="project",
-    )(normed, own, other)
+    )(normed, *stacks)
 
 
 def pair_masks():
@@ -222,20 +267,17 @@
         scratch_shapes=[pltpu.VMEM((HV, HK), F32)],
         compiler_params=limit(6),
         name="state",
-    )(fv, run, tail, gap, state)
-
-
-def local_kernel(a_ref, own_ref, other_ref, fv_ref, gap_ref, out_ref):
-    half = own_ref.shape[0]
+    )(fv, in_hbm(run), in_hbm(tail), in_hbm(gap), in_hbm(state))
+
+
+def local_kernel(a_ref, fv_ref, gap_ref, *refs):
+    out_ref, stacks = refs[-1], refs[:-1]
     seqs, heads, _, _, _ = fv_ref.shape
     wide = heads * HK
     causal, _, _ = pair_masks()
     ones = causal.astype(F32).astype(BF16)
-    total_q = dot(a_ref[:, :half], own_ref[:, :wide]) + dot(a_ref[:, half:], other_ref[:, :wide])
-    q_pre = total_q.astype(BF16)
-    total_g = dot(a_ref[:, :half], own_ref[:, wide : 2 * wide])
-    total_g += dot(a_ref[:, half:], other_ref[:, wide : 2 * wide])
-    g_pre = total_g.astype(BF16)
+    q_pre = against(a_ref, stacks, slice(0, wide)).astype(BF16)
+    g_pre = against(a_ref, stacks, slice(wide, 2 * wide)).astype(BF16)
     for p in range(seqs // 2):
         for h in range(heads):
             q = q_pre[p * PAIR : (p + 1) * PAIR, h * HK : (h + 1) * HK].astype(F32)
@@ -248,38 +290,38 @@
             out_ref[2, p, h] = g_pre[p * PAIR : (p + 1) * PAIR, h * HV : (h + 1) * HV]
 
 
-def weight_kernel(where_ref, own_ref, other_ref, weight_ref):
-    wide = HEADS * HV
-    for k, stack in enumerate((own_ref, other_ref)):
-        for j in range(len(OFFSETS)):
-            start = pl.multiple_of(place(where_ref, k * len(OFFSETS) + j) * OUT_ROWS, OUT_ROWS)
+def weight_kernel(where_ref, *refs):
+    weight_ref = refs[-1]
+    j = 0
+    for stack in refs[:-1]:
+        for first in range(0, stack.shape[0], ROWS):
+            start = pl.multiple_of(place(where_ref, j) * OUT_ROWS, OUT_ROWS)
             for n in range(ROWS // OUT_ROWS):
-                first = j * ROWS + n * OUT_ROWS
-                weight_ref[pl.ds(start, OUT_ROWS), n * wide : (n + 1) * wide] = stack[
-                    first : first + OUT_ROWS, 2 * wide :
-                ]
-
-
-def local_parts(normed, own, other, fv, gap):
+                rows = slice(first + n * OUT_ROWS, first + (n + 1) * OUT_ROWS)
+                weight_ref[pl.ds(start, OUT_ROWS), n * WIDE : (n + 1) * WIDE] = stack[rows, 2 * WIDE :]
+            j += 1
+
+
+def local_parts(normed, stacks, fv, gap):
     seqs, heads, _, _, _ = fv.shape
     return pl.pallas_call(
         local_kernel,
-        in_specs=[vmem_spec()] * 5,
+        in_specs=[vmem_spec()] * (3 + len(stacks)),
         out_shape=pltpu.HBM((3, seqs // 2, heads, PAIR, HK), BF16),
         compiler_params=limit(14),
         name="local",
-    )(normed, own, other, fv, gap)
-
-
-def out_weight(where, own, other, width):
+    )(normed, fv, gap, *stacks)
+
+
+def out_weight(where, stacks, width):
     return pl.pallas_call(
         weight_kernel,
-        in_specs=[pl.BlockSpec(memory_space=pltpu.SMEM)] + [vmem_spec()] * 2,
+        in_specs=[pl.BlockSpec(memory_space=pltpu.SMEM)] + [vmem_spec()] * len(stacks),
         out_specs=vmem_spec(),
-        out_shape=jax.ShapeDtypeStruct((HEADS * HV, width), BF16),
+        out_shape=jax.ShapeDtypeStruct((WIDE, width), BF16),
         compiler_params=limit(4),
         name="weight",
-    )(where, own, other)
+    )(where, *stacks)
 
 
 def output_kernel(state_ref, part_ref, fv_ref, weight_ref, norm_ref, post_ref, out_ref):
@@ -334,7 +376,7 @@
         out_shape=jax.ShapeDtypeStruct((seqs, local_len, width), BF16),
         compiler_params=limit(12),
         name="output",
-    )(states, parts, fv, weight, norm_gain.reshape(1, HV), post_gain.reshape(1, width))
+    )(states, in_hbm(parts), in_hbm(fv), weight, norm_gain.reshape(1, HV), post_gain.reshape(1, width))
 
 
 def layer(
@@ -353,13 +395,13 @@
 ):
     seqs, local_len, width = tokens.shape
     items = seqs * HEADS
-    wide = HEADS * HV
     where = jnp.stack([lax.axis_index("y"), lax.axis_index("c")]).astype(jnp.int32)
     gaps = (1.0 - lower_bound).reshape(HEADS, HK)
 
-    first = jnp.concatenate([w_forget, w_value], axis=1)
-    stacked = [w_out[:, n * wide : (n + 1) * wide] for n in range(width // wide)]
-    second = jnp.concatenate([w_query, w_gate, jnp.concatenate(stacked, axis=0)], axis=1)
+    first = joined((w_forget, w_value), ((0, (0, 0), (0, 0)), (1, (0, 0), (0, WIDE))), 2 * WIDE)
+    places = [(0, (0, 0), (0, 0)), (1, (0, 0), (0, WIDE))]
+    places += [(2, (0, n * WIDE), (n * OUT_ROWS, 2 * WIDE)) for n in range(width // WIDE)]
+    second = joined((w_query, w_gate, w_out), tuple(places), 3 * WIDE)
     gap = lax.dynamic_slice_in_dim(gaps, lax.axis_index("x"), 1, 0)
     run = jnp.cumsum(extra_decay.reshape(items, CHUNK), axis=1)
     high = lax.reduce_precision(run, 8, 7)
@@ -371,18 +413,16 @@
     state = initial_state[0].T
     normed = normed_tokens(tokens.reshape(seqs * local_len, width), pre_gain, where)
 
-    early = (second, gap, run, tail, state, normed)
-    first_own = gathered_y(first, ((), (), early, ()))
-    first_other = swapped(first_own)
-    fv = project_heads(normed, first_own, first_other, seqs, local_len)
+    first_own, first_other = gathered_y(first, ((), (normed,), (second,), ()))
+    fv = project_heads(normed, first_own + first_other, seqs, local_len)
     moved = lax.all_to_all(fv.reshape(items, 2 * local_len, HK), SP, 0, 0, tiled=True)
     starts = chunk_states(moved.reshape(items, 2, local_len, HK), run, tail, gap, state)
     states = lax.all_to_all(starts, SP, 0, 0, tiled=True)
 
-    second_own = gathered_y(second, ((first_own,), (fv,), (), (starts,)))
-    second_other = swapped(second_own)
-    parts = local_parts(normed, second_own, second_other, fv, gaps)
-    weight = out_weight(where, second_own, second_other, width)
+    second_own, second_other = gathered_y(second, ((), (), (), ()))
+    stacks = second_own + second_other
+    parts = local_parts(normed, stacks, fv, gaps)
+    weight = out_weight(where, stacks, width)
     states = states.reshape(seqs, HEADS, HV + TAIL, HK)
     return output_rows(states, parts, fv, weight, norm_gain, post_gain)
 

time: 186 us -> 171 us (0.919)
  local copies, waits for them, and re-layouts: 20.6 us -> 8.17 us
  waiting for transfers between devices: 45.3 us -> 39.8 us
  starting transfers between devices: 91.8 us -> 87.3 us
  Pallas kernels: 23.3 us -> 27.5 us
  other arithmetic: 2.48 us -> 5.97 us
    all_to_all x1, waiting for transfers between devices: 15.8 us -> 0.01 us  [layer(): states = lax.all_to_all(starts, SP, 0, 0, tiled=True)]
    unnamed x53 -> x12, local copies, waits for them, and re-layouts: 18.5 us -> 2.79 us
    ppermute x16 -> x14, waiting for transfers between devices: 25.7 us -> 37.4 us  [shifted(): return lax.ppermute(a, 'y', [(i, (i + step) % size) for i in range(size)])]
    ppermute x16 -> x14, starting transfers between devices: 55.9 us -> 45.2 us  [shifted(): return lax.ppermute(a, 'y', [(i, (i + step) % size) for i in range(size)])]
    ppermute x2 -> x6, starting transfers between devices: 15.3 us -> 22.2 us  [swapped(): return lax.ppermute(a, 'c', [(0, 1), (1, 0)])]
    another operation x3, local copies, waits for them, and re-layouts: 0.15 us -> 2.79 us  [layer(): jnp.stack([high, middle, low] + [jnp.zeros_like(high)] * (TAIL - 3), axis=1)]
    ppermute x2 -> x6, waiting for transfers between devices: 3.77 us -> 2.46 us  [swapped(): return lax.ppermute(a, 'c', [(0, 1), (1, 0)])]
    pallas_call x2 -> x4, Pallas kernels: 10.4 us -> 11.5 us  [the longest x1 5.3 us: local_parts(): pl.pallas_call(local_kernel, in_specs=[vmem_spec()] * (3 + len(stacks)),...]
  transfers between devices with their start and end apart: 20 -> 22, of which waited for: 13 -> 9; matrix products, arithmetic and copies ran while one was open for 3% -> 8% of each run, Pallas kernels for 7% -> 10%
where the time goes in v1:
time: 171 us; the launch traced here: 169 us
  starting transfers between devices  87.3 us (51%)
  waiting for transfers between devices  39.8 us (23%)
  Pallas kernels  27.5 us (16%)
  local copies, waits for them, and re-layouts  8.17 us (5%)
  other arithmetic  5.97 us (3%)
    ppermute x14, starting transfers between devices, shifted(): return lax.ppermute(a, 'y', [(i, (i + step) % size) for i in range(size)])  45.2 us
    ppermute x14, waiting for transfers between devices, shifted(): return lax.ppermute(a, 'y', [(i, (i + step) % size) for i in range(size)])  37.4 us
    ppermute x6, starting transfers between devices, swapped(): return lax.ppermute(a, 'c', [(0, 1), (1, 0)])  22.2 us
    all_to_all x1, starting transfers between devices, layer(): lax.all_to_all(fv.reshape(items, 2 * local_len, HK), SP, 0, 0, tiled=True)  10.6 us
    all_to_all x1, starting transfers between devices, layer(): states = lax.all_to_all(starts, SP, 0, 0, tiled=True)  9.33 us
    pallas_call x1, Pallas kernels, output_rows(): pl.pallas_call(output_kernel, grid=(seqs // group,), in_specs=[vmem_spec(...  5.77 us
    pallas_call x1, Pallas kernels, local_parts(): pl.pallas_call(local_kernel, in_specs=[vmem_spec()] * (3 + len(stacks)),...  5.3 us
    pallas_call x1, Pallas kernels, project_heads(): pl.pallas_call(project_kernel, grid=(HEADS,), in_specs=[vmem_spec()] * (1...  4.2 us
  transfers between devices with their start and end apart: 22, of which 9 were waited for; matrix products, arithmetic and copies ran while one was open for 8% of the time, Pallas kernels for 10%

profile of v1, /device:TPU:1, one launch (start us, length us, event | category | flops | bytes accessed | tf_op | source)
XLA Modules:
  0.0 169.1 jit_solution(15815980032149270902)
XLA Ops:
  1.0 4.0 %collective-permute-start = (bf16[128,1024]{1,0:T(8,128)(2,1)S(1)}, bf16[128,1024]{1,0:T(8,128)(2,1)S(1)}, u32[]{:S(2)}, u32[]{:S(2)}) collective-permute-start(bf16[128,1024]{1,0:T(8,128)(2,1)S(1)} %shard_map.118.refs_0_), channel_id=1, source_target_pairs={{0,2},{2,4},{4,6},{6,8},{8,10},{10,12},{12,14},{14,0},{1,3},{3,5},... | collective-permute-start | bytes 786440 | tf_op jit(solution)/shard_map/ppermute | solution.py:34
  5.0 3.8 %collective-permute-start.1 = (bf16[128,1024]{1,0:T(8,128)(2,1)S(1)}, bf16[128,1024]{1,0:T(8,128)(2,1)S(1)}, u32[]{:S(2)}, u32[]{:S(2)}) collective-permute-start(bf16[128,1024]{1,0:T(8,128)(2,1)S(1)} %shard_map.118.refs_0_), channel_id=1, source_target_pairs={{0,14},{2,0},{4,2},{6,4},{8,6},{10,8},{12,10},{14,12},{1,15},{3,1}... | collective-permute-start | bytes 786440 | tf_op jit(solution)/shard_map/ppermute | solution.py:34
  9.6 3.6 %norm.1.a_ref = bf16[512,2048]{1,0:T(8,128)(2,1)S(1)} custom-call(s32[2]{0:T(128)S(1)} %pad_add_fusion.where_ref, bf16[512,2048]{1,0:T(8,128)(2,1)} %bitcast.20, f32[1,2048]{1,0:T(1,128)S(1)} %bitcast.17), custom_call_target="tpu_custom_call" | custom-call | tf_op jit(solution)/shard_map/norm/pallas_call | solution.py:157
  13.2 3.8 %collective-permute-start.2 = (bf16[128,1024]{1,0:T(8,128)(2,1)S(1)}, bf16[128,1024]{1,0:T(8,128)(2,1)S(1)}, u32[]{:S(2)}, u32[]{:S(2)}) collective-permute-start(bf16[128,1024]{1,0:T(8,128)(2,1)S(1)} %collective-permute-done.refs_1_), channel_id=1, source_target_pairs={{0,2},{2,4},{4,6},{6,8},{8,10},{10,12},{12,14},{14,0},{1,3},{3,5},... | collective-permute-start | bytes 786440 | tf_op jit(solution)/shard_map/ppermute | solution.py:34
  21.6 4.1 %collective-permute-done.3.refs_4_ = bf16[128,1024]{1,0:T(8,128)(2,1)S(1)} collective-permute-done((bf16[128,1024]{1,0:T(8,128)(2,1)S(1)}, bf16[128,1024]{1,0:T(8,128)(2,1)S(1)}, u32[]{:S(2)}, u32[]{:S(2)}) %collective-permute-start.3) | collective-permute-done | bytes 262176 | tf_op jit(solution)/shard_map/ppermute | solution.py:34
  25.7 6.5 %collective-permute-start.7 = (bf16[640,1024]{1,0:T(8,128)(2,1)S(1)}, bf16[640,1024]{1,0:T(8,128)(2,1)S(1)}, u32[]{:S(2)}, u32[]{:S(2)}) collective-permute-start(bf16[640,1024]{1,0:T(8,128)(2,1)S(1)} %stack.27.refs_0_), channel_id=1, source_target_pairs={{0,1},{1,0},{2,3},{3,2},{4,5},{5,4},{6,7},{7,6},{8,9},{9,8},{10,11... | collective-permute-start | bytes 3932168 | tf_op jit(solution)/shard_map/ppermute | solution.py:38
  33.3 2.9 %collective-permute-start.4 = (bf16[128,1024]{1,0:T(8,128)(2,1)S(1)}, bf16[128,1024]{1,0:T(8,128)(2,1)S(1)}, u32[]{:S(2)}, u32[]{:S(2)}) collective-permute-start(bf16[128,1024]{1,0:T(8,128)(2,1)S(1)} %collective-permute-done.2.refs_3_), channel_id=1, source_target_pairs={{0,2},{2,4},{4,6},{6,8},{8,10},{10,12},{12,14},{14,0},{1,3},{3,5},... | collective-permute-start | bytes 786440 | tf_op jit(solution)/shard_map/ppermute | solution.py:34
  36.2 4.4 %collective-permute-start.5 = (bf16[128,1024]{1,0:T(8,128)(2,1)S(1)}, bf16[128,1024]{1,0:T(8,128)(2,1)S(1)}, u32[]{:S(2)}, u32[]{:S(2)}) collective-permute-start(bf16[128,1024]{1,0:T(8,128)(2,1)S(1)} %collective-permute-done.3.refs_4_), channel_id=1, source_target_pairs={{0,14},{2,0},{4,2},{6,4},{8,6},{10,8},{12,10},{14,12},{1,15},{3,1}... | collective-permute-start | bytes 786440 | tf_op jit(solution)/shard_map/ppermute | solution.py:34
  40.5 4.7 %collective-permute-done.4.refs_0_ = bf16[128,1024]{1,0:T(8,128)(2,1)S(1)} collective-permute-done((bf16[128,1024]{1,0:T(8,128)(2,1)S(1)}, bf16[128,1024]{1,0:T(8,128)(2,1)S(1)}, u32[]{:S(2)}, u32[]{:S(2)}) %collective-permute-start.4) | collective-permute-done | bytes 262176 | tf_op jit(solution)/shard_map/ppermute | solution.py:34
  49.7 5.9 %collective-permute-done.6.refs_2_ = bf16[128,1024]{1,0:T(8,128)(2,1)S(1)} collective-permute-done((bf16[128,1024]{1,0:T(8,128)(2,1)S(1)}, bf16[128,1024]{1,0:T(8,128)(2,1)S(1)}, u32[]{:S(2)}, u32[]{:S(2)}) %collective-permute-start.6) | collective-permute-done | bytes 262176 | tf_op jit(solution)/shard_map/ppermute | solution.py:34
  55.6 3.3 %collective-permute-start.9 = (bf16[128,1024]{1,0:T(8,128)(2,1)S(1)}, bf16[128,1024]{1,0:T(8,128)(2,1)S(1)}, u32[]{:S(2)}, u32[]{:S(2)}) collective-permute-start(bf16[128,1024]{1,0:T(8,128)(2,1)S(1)} %collective-permute-done.6.refs_2_), channel_id=1, source_target_pairs={{0,1},{1,0},{2,3},{3,2},{4,5},{5,4},{6,7},{7,6},{8,9},{9,8},{10,11... | collective-permute-start | bytes 786440 | tf_op jit(solution)/shard_map/ppermute | solution.py:38
  60.1 4.2 %project.1.fv_ref = bf16[8,4,2,64,128]{4,3,2,1,0:T(8,128)(2,1)} custom-call(bf16[512,2048]{1,0:T(8,128)(2,1)S(1)} %norm.1.a_ref, bf16[640,1024]{1,0:T(8,128)(2,1)S(1)} %stack.27.refs_0_, bf16[256,1024]{1,0:T(8,128)(2,1)S(1)} %stack.28.refs_1_, bf16[128,1024]{1,0:T(8,128)(2,1)S(1)} %collective-permute-done.6.refs_2_, ...), custom_call_target="tpu_custom_call" | custom-call | tf_op jit(solution)/shard_map/project/pallas_call | solution.py:194
  64.3 10.6 %all-to-all-start = ((bf16[32,128,128]{2,1,0:T(8,128)(2,1)}), bf16[32,128,128]{2,1,0:T(8,128)(2,1)S(1)}, u32[]{:S(2)}, u32[]{:S(2)}) async-start(bf16[32,128,128]{2,1,0:T(8,128)(2,1)} %bitcast.15), calls=%async_computation | async-start | bytes 2097152 | tf_op jit(solution)/shard_map/all_to_all | solution.py:418
  76.8 4.6 %collective-permute-start.11 = (bf16[128,1536]{1,0:T(8,128)(2,1)S(1)}, bf16[128,1536]{1,0:T(8,128)(2,1)}, u32[]{:S(2)}, u32[]{:S(2)}) collective-permute-start(bf16[128,1536]{1,0:T(8,128)(2,1)S(1)} %shard_map.119.refs_0_), channel_id=1, source_target_pairs={{0,14},{2,0},{4,2},{6,4},{8,6},{10,8},{12,10},{14,12},{1,15},{3,1}... | collective-permute-start | bytes 1179656 | tf_op jit(solution)/shard_map/ppermute | solution.py:34
  94.6 4.6 %collective-permute-start.13 = (bf16[128,1536]{1,0:T(8,128)(2,1)}, bf16[128,1536]{1,0:T(8,128)(2,1)}, u32[]{:S(2)}, u32[]{:S(2)}) collective-permute-start(bf16[128,1536]{1,0:T(8,128)(2,1)} %collective-permute-done.11.refs_2_), channel_id=1, source_target_pairs={{0,14},{2,0},{4,2},{6,4},{8,6},{10,8},{12,10},{14,12},{1,15},{3,1}... | collective-permute-start | bytes 1179656 | tf_op jit(solution)/shard_map/ppermute | solution.py:34
  101.3 4.2 %state.1 = bf16[32,136,128]{2,1,0:T(8,128)(2,1)} custom-call(bf16[32,2,64,128]{3,2,1,0:T(8,128)(2,1)S(1)} %bitcast.16, f32[16,128]{1,0:T(8,128)} %reshape.59.run_ref, bf16[32,8,128]{2,1,0:T(8,128)(2,1)} %pad_maximum_fusion.tail_ref, f32[1,128]{1,0:T(1,128)} %constant_dynamic-slice_fusion.gap_ref, f32[128,128]{1,0:T(8,128)} %bitcast.21), custom_call_target="tpu_custom_call" | custom-call | tf_op jit(solution)/shard_map/state/pallas_call | solution.py:255
  105.5 9.3 %all-to-all-start.1 = ((bf16[32,136,128]{2,1,0:T(8,128)(2,1)}), bf16[32,136,128]{2,1,0:T(8,128)(2,1)}, u32[]{:S(2)}, u32[]{:S(2)}) async-start(bf16[32,136,128]{2,1,0:T(8,128)(2,1)} %state.1), calls=%async_computation.1 | async-start | bytes 2228224 | tf_op jit(solution)/shard_map/all_to_all | solution.py:420
  116.5 4.2 %collective-permute-start.17 = (bf16[640,1536]{1,0:T(8,128)(2,1)S(1)}, bf16[640,1536]{1,0:T(8,128)(2,1)S(1)}, u32[]{:S(2)}, u32[]{:S(2)}) collective-permute-start(bf16[640,1536]{1,0:T(8,128)(2,1)S(1)} %stack.29.refs_0_), channel_id=1, source_target_pairs={{0,1},{1,0},{2,3},{3,2},{4,5},{5,4},{6,7},{7,6},{8,9},{9,8},{10,11... | collective-permute-start | bytes 5898248 | tf_op jit(solution)/shard_map/ppermute | solution.py:38
  122.6 4.6 %collective-permute-start.15 = (bf16[128,1536]{1,0:T(8,128)(2,1)}, bf16[128,1536]{1,0:T(8,128)(2,1)S(1)}, u32[]{:S(2)}, u32[]{:S(2)}) collective-permute-start(bf16[128,1536]{1,0:T(8,128)(2,1)} %collective-permute-done.13.refs_4_), channel_id=1, source_target_pairs={{0,14},{2,0},{4,2},{6,4},{8,6},{10,8},{12,10},{14,12},{1,15},{3,1}... | collective-permute-start | bytes 1179656 | tf_op jit(solution)/shard_map/ppermute | solution.py:34
  127.2 7.6 %collective-permute-done.14.refs_0_ = bf16[128,1536]{1,0:T(8,128)(2,1)S(1)} collective-permute-done((bf16[128,1536]{1,0:T(8,128)(2,1)}, bf16[128,1536]{1,0:T(8,128)(2,1)S(1)}, u32[]{:S(2)}, u32[]{:S(2)}) %collective-permute-start.14) | collective-permute-done | bytes 393248 | tf_op jit(solution)/shard_map/ppermute | solution.py:34
  135.7 3.1 %collective-permute-start.18 = (bf16[256,1536]{1,0:T(8,128)(2,1)S(1)}, bf16[256,1536]{1,0:T(8,128)(2,1)S(1)}, u32[]{:S(2)}, u32[]{:S(2)}) collective-permute-start(bf16[256,1536]{1,0:T(8,128)(2,1)S(1)} %stack.30.refs_1_), channel_id=1, source_target_pairs={{0,1},{1,0},{2,3},{3,2},{4,5},{5,4},{6,7},{7,6},{8,9},{9,8},{10,11... | collective-permute-start | bytes 2359304 | tf_op jit(solution)/shard_map/ppermute | solution.py:38
  141.1 12.4 %collective-permute-done.16.refs_2_ = bf16[128,1536]{1,0:T(8,128)(2,1)S(1)} collective-permute-done((bf16[128,1536]{1,0:T(8,128)(2,1)S(1)}, bf16[128,1536]{1,0:T(8,128)(2,1)S(1)}, u32[]{:S(2)}, u32[]{:S(2)}) %collective-permute-start.16) | collective-permute-done | bytes 393248 | tf_op jit(solution)/shard_map/ppermute | solution.py:34
  157.3 5.3 %local.1.part_ref = bf16[3,4,4,128,128]{4,3,2,1,0:T(8,128)(2,1)} custom-call(bf16[512,2048]{1,0:T(8,128)(2,1)S(1)} %norm.1.a_ref, bf16[8,4,2,64,128]{4,3,2,1,0:T(8,128)(2,1)S(1)} %copy-done, f32[4,128]{1,0:T(4,128)S(1)} %subtract_bitcast_fusion.gap_ref, bf16[640,1536]{1,0:T(8,128)(2,1)S(1)} %stack.29.refs_0_, bf16[256,1536]{1,0:T(8,128)(2,1)S(1)} %stack.30.refs_1_, ...), custom_call_target="tpu_custom_call" | custom-call | tf_op jit(solution)/shard_map/local/pallas_call | solution.py:307
  163.3 5.8 %output.1 = bf16[8,64,2048]{2,1,0:T(8,128)(2,1)} custom-call(bf16[8,4,136,128]{3,2,1,0:T(8,128)(2,1)} %bitcast.10.state_ref, bf16[3,4,4,128,128]{4,3,2,1,0:T(8,128)(2,1)} %local.1.part_ref, bf16[8,4,2,64,128]{4,3,2,1,0:T(8,128)(2,1)} %project.1.fv_ref, bf16[512,2048]{1,0:T(8,128)(2,1)S(1)} %weight.1.weight_ref, f32[1,128]{1,0:T(1,128)S(1)} %bitcast.19, ...), custom_call_target="tpu_custom_call" | custom-call | tf_op jit(solution)/shard_map/output/pallas_call | solution.py:364
  (56 shorter events, 41.4 us)
Async XLA Ops:
  1.0 12.2 %collective-permute-start = (bf16[128,1024]{1,0:T(8,128)(2,1)S(1)}, bf16[128,1024]{1,0:T(8,128)(2,1)S(1)}, u32[]{:S(2)}, u32[]{:S(2)}) collective-permute-start(bf16[128,1024]{1,0:T(8,128)(2,1)S(1)} %shard_map.118.refs_0_), channel_id=1, source_target_pairs={{0,2},{2,4},{4,6},{6,8},{8,10},{10,12},{12,14},{14,0},{1,3},{3,5},... | collective-permute-start | bytes 786440 | tf_op jit(solution)/shard_map/ppermute | solution.py:34
  5.0 8.2 %collective-permute-start.1 = (bf16[128,1024]{1,0:T(8,128)(2,1)S(1)}, bf16[128,1024]{1,0:T(8,128)(2,1)S(1)}, u32[]{:S(2)}, u32[]{:S(2)}) collective-permute-start(bf16[128,1024]{1,0:T(8,128)(2,1)S(1)} %shard_map.118.refs_0_), channel_id=1, source_target_pairs={{0,14},{2,0},{4,2},{6,4},{8,6},{10,8},{12,10},{14,12},{1,15},{3,1}... | collective-permute-start | bytes 786440 | tf_op jit(solution)/shard_map/ppermute | solution.py:34
  13.2 8.3 %collective-permute-start.2 = (bf16[128,1024]{1,0:T(8,128)(2,1)S(1)}, bf16[128,1024]{1,0:T(8,128)(2,1)S(1)}, u32[]{:S(2)}, u32[]{:S(2)}) collective-permute-start(bf16[128,1024]{1,0:T(8,128)(2,1)S(1)} %collective-permute-done.refs_1_), channel_id=1, source_target_pairs={{0,2},{2,4},{4,6},{6,8},{8,10},{10,12},{12,14},{14,0},{1,3},{3,5},... | collective-permute-start | bytes 786440 | tf_op jit(solution)/shard_map/ppermute | solution.py:34
  17.0 8.6 %collective-permute-start.3 = (bf16[128,1024]{1,0:T(8,128)(2,1)S(1)}, bf16[128,1024]{1,0:T(8,128)(2,1)S(1)}, u32[]{:S(2)}, u32[]{:S(2)}) collective-permute-start(bf16[128,1024]{1,0:T(8,128)(2,1)S(1)} %collective-permute-done.1.refs_2_), channel_id=1, source_target_pairs={{0,14},{2,0},{4,2},{6,4},{8,6},{10,8},{12,10},{14,12},{1,15},{3,1}... | collective-permute-start | bytes 786440 | tf_op jit(solution)/shard_map/ppermute | solution.py:34
  25.7 34.4 %collective-permute-start.7 = (bf16[640,1024]{1,0:T(8,128)(2,1)S(1)}, bf16[640,1024]{1,0:T(8,128)(2,1)S(1)}, u32[]{:S(2)}, u32[]{:S(2)}) collective-permute-start(bf16[640,1024]{1,0:T(8,128)(2,1)S(1)} %stack.27.refs_0_), channel_id=1, source_target_pairs={{0,1},{1,0},{2,3},{3,2},{4,5},{5,4},{6,7},{7,6},{8,9},{9,8},{10,11... | collective-permute-start | bytes 3932168 | tf_op jit(solution)/shard_map/ppermute | solution.py:38
  33.3 12.0 %collective-permute-start.4 = (bf16[128,1024]{1,0:T(8,128)(2,1)S(1)}, bf16[128,1024]{1,0:T(8,128)(2,1)S(1)}, u32[]{:S(2)}, u32[]{:S(2)}) collective-permute-start(bf16[128,1024]{1,0:T(8,128)(2,1)S(1)} %collective-permute-done.2.refs_3_), channel_id=1, source_target_pairs={{0,2},{2,4},{4,6},{6,8},{8,10},{10,12},{12,14},{14,0},{1,3},{3,5},... | collective-permute-start | bytes 786440 | tf_op jit(solution)/shard_map/ppermute | solution.py:34
  36.2 11.0 %collective-permute-start.5 = (bf16[128,1024]{1,0:T(8,128)(2,1)S(1)}, bf16[128,1024]{1,0:T(8,128)(2,1)S(1)}, u32[]{:S(2)}, u32[]{:S(2)}) collective-permute-start(bf16[128,1024]{1,0:T(8,128)(2,1)S(1)} %collective-permute-done.3.refs_4_), channel_id=1, source_target_pairs={{0,14},{2,0},{4,2},{6,4},{8,6},{10,8},{12,10},{14,12},{1,15},{3,1}... | collective-permute-start | bytes 786440 | tf_op jit(solution)/shard_map/ppermute | solution.py:34
  45.2 10.4 %collective-permute-start.6 = (bf16[128,1024]{1,0:T(8,128)(2,1)S(1)}, bf16[128,1024]{1,0:T(8,128)(2,1)S(1)}, u32[]{:S(2)}, u32[]{:S(2)}) collective-permute-start(bf16[128,1024]{1,0:T(8,128)(2,1)S(1)} %collective-permute-done.4.refs_0_), channel_id=1, source_target_pairs={{0,2},{2,4},{4,6},{6,8},{8,10},{10,12},{12,14},{14,0},{1,3},{3,5},... | collective-permute-start | bytes 786440 | tf_op jit(solution)/shard_map/ppermute | solution.py:34
  47.2 11.8 %collective-permute-start.8 = (bf16[256,1024]{1,0:T(8,128)(2,1)S(1)}, bf16[256,1024]{1,0:T(8,128)(2,1)S(1)}, u32[]{:S(2)}, u32[]{:S(2)}) collective-permute-start(bf16[256,1024]{1,0:T(8,128)(2,1)S(1)} %stack.28.refs_1_), channel_id=1, source_target_pairs={{0,1},{1,0},{2,3},{3,2},{4,5},{5,4},{6,7},{7,6},{8,9},{9,8},{10,11... | collective-permute-start | bytes 1572872 | tf_op jit(solution)/shard_map/ppermute | solution.py:38
  55.6 4.5 %collective-permute-start.9 = (bf16[128,1024]{1,0:T(8,128)(2,1)S(1)}, bf16[128,1024]{1,0:T(8,128)(2,1)S(1)}, u32[]{:S(2)}, u32[]{:S(2)}) collective-permute-start(bf16[128,1024]{1,0:T(8,128)(2,1)S(1)} %collective-permute-done.6.refs_2_), channel_id=1, source_target_pairs={{0,1},{1,0},{2,3},{3,2},{4,5},{5,4},{6,7},{7,6},{8,9},{9,8},{10,11... | collective-permute-start | bytes 786440 | tf_op jit(solution)/shard_map/ppermute | solution.py:38
  64.3 28.3 %copy-start.4 = (f32[512]{0:T(512)S(1)}, f32[512]{0:T(512)}, u32[]{:S(2)}) copy-start(f32[512]{0:T(512)} %param.18) | copy-start | bytes 6148
  64.3 37.0 %all-to-all-start = ((bf16[32,128,128]{2,1,0:T(8,128)(2,1)}), bf16[32,128,128]{2,1,0:T(8,128)(2,1)S(1)}, u32[]{:S(2)}, u32[]{:S(2)}) async-start(bf16[32,128,128]{2,1,0:T(8,128)(2,1)} %bitcast.15), calls=%async_computation | async-start | bytes 2097152 | tf_op jit(solution)/shard_map/all_to_all | solution.py:418
  74.9 17.7 %collective-permute-start.10 = (bf16[128,1536]{1,0:T(8,128)(2,1)S(1)}, bf16[128,1536]{1,0:T(8,128)(2,1)}, u32[]{:S(2)}, u32[]{:S(2)}) collective-permute-start(bf16[128,1536]{1,0:T(8,128)(2,1)S(1)} %shard_map.119.refs_0_), channel_id=1, source_target_pairs={{0,2},{2,4},{4,6},{6,8},{8,10},{10,12},{12,14},{14,0},{1,3},{3,5},... | collective-permute-start | bytes 1179656 | tf_op jit(solution)/shard_map/ppermute | solution.py:34
  76.8 17.7 %collective-permute-start.11 = (bf16[128,1536]{1,0:T(8,128)(2,1)S(1)}, bf16[128,1536]{1,0:T(8,128)(2,1)}, u32[]{:S(2)}, u32[]{:S(2)}) collective-permute-start(bf16[128,1536]{1,0:T(8,128)(2,1)S(1)} %shard_map.119.refs_0_), channel_id=1, source_target_pairs={{0,14},{2,0},{4,2},{6,4},{8,6},{10,8},{12,10},{14,12},{1,15},{3,1}... | collective-permute-start | bytes 1179656 | tf_op jit(solution)/shard_map/ppermute | solution.py:34
  92.6 22.2 %collective-permute-start.12 = (bf16[128,1536]{1,0:T(8,128)(2,1)}, bf16[128,1536]{1,0:T(8,128)(2,1)}, u32[]{:S(2)}, u32[]{:S(2)}) collective-permute-start(bf16[128,1536]{1,0:T(8,128)(2,1)} %collective-permute-done.10.refs_1_), channel_id=1, source_target_pairs={{0,2},{2,4},{4,6},{6,8},{8,10},{10,12},{12,14},{14,0},{1,3},{3,5},... | collective-permute-start | bytes 1179656 | tf_op jit(solution)/shard_map/ppermute | solution.py:34
  94.6 20.3 %collective-permute-start.13 = (bf16[128,1536]{1,0:T(8,128)(2,1)}, bf16[128,1536]{1,0:T(8,128)(2,1)}, u32[]{:S(2)}, u32[]{:S(2)}) collective-permute-start(bf16[128,1536]{1,0:T(8,128)(2,1)} %collective-permute-done.11.refs_2_), channel_id=1, source_target_pairs={{0,14},{2,0},{4,2},{6,4},{8,6},{10,8},{12,10},{14,12},{1,15},{3,1}... | collective-permute-start | bytes 1179656 | tf_op jit(solution)/shard_map/ppermute | solution.py:34
  105.5 57.8 %all-to-all-start.1 = ((bf16[32,136,128]{2,1,0:T(8,128)(2,1)}), bf16[32,136,128]{2,1,0:T(8,128)(2,1)}, u32[]{:S(2)}, u32[]{:S(2)}) async-start(bf16[32,136,128]{2,1,0:T(8,128)(2,1)} %state.1), calls=%async_computation.1 | async-start | bytes 2228224 | tf_op jit(solution)/shard_map/all_to_all | solution.py:420
  114.9 42.5 %copy-start = (bf16[8,4,2,64,128]{4,3,2,1,0:T(8,128)(2,1)S(1)}, bf16[8,4,2,64,128]{4,3,2,1,0:T(8,128)(2,1)}, u32[]{:S(2)}) copy-start(bf16[8,4,2,64,128]{4,3,2,1,0:T(8,128)(2,1)} %project.1.fv_ref) | copy-start | bytes 3145732
  116.5 40.9 %collective-permute-start.17 = (bf16[640,1536]{1,0:T(8,128)(2,1)S(1)}, bf16[640,1536]{1,0:T(8,128)(2,1)S(1)}, u32[]{:S(2)}, u32[]{:S(2)}) collective-permute-start(bf16[640,1536]{1,0:T(8,128)(2,1)S(1)} %stack.29.refs_0_), channel_id=1, source_target_pairs={{0,1},{1,0},{2,3},{3,2},{4,5},{5,4},{6,7},{7,6},{8,9},{9,8},{10,11... | collective-permute-start | bytes 5898248 | tf_op jit(solution)/shard_map/ppermute | solution.py:38
  120.7 14.1 %collective-permute-start.14 = (bf16[128,1536]{1,0:T(8,128)(2,1)}, bf16[128,1536]{1,0:T(8,128)(2,1)S(1)}, u32[]{:S(2)}, u32[]{:S(2)}) collective-permute-start(bf16[128,1536]{1,0:T(8,128)(2,1)} %collective-permute-done.12.refs_3_), channel_id=1, source_target_pairs={{0,2},{2,4},{4,6},{6,8},{8,10},{10,12},{12,14},{14,0},{1,3},{3,5},... | collective-permute-start | bytes 1179656 | tf_op jit(solution)/shard_map/ppermute | solution.py:34
  122.6 13.1 %collective-permute-start.15 = (bf16[128,1536]{1,0:T(8,128)(2,1)}, bf16[128,1536]{1,0:T(8,128)(2,1)S(1)}, u32[]{:S(2)}, u32[]{:S(2)}) collective-permute-start(bf16[128,1536]{1,0:T(8,128)(2,1)} %collective-permute-done.13.refs_4_), channel_id=1, source_target_pairs={{0,14},{2,0},{4,2},{6,4},{8,6},{10,8},{12,10},{14,12},{1,15},{3,1}... | collective-permute-start | bytes 1179656 | tf_op jit(solution)/shard_map/ppermute | solution.py:34
  135.7 20.3 %collective-permute-start.18 = (bf16[256,1536]{1,0:T(8,128)(2,1)S(1)}, bf16[256,1536]{1,0:T(8,128)(2,1)S(1)}, u32[]{:S(2)}, u32[]{:S(2)}) collective-permute-start(bf16[256,1536]{1,0:T(8,128)(2,1)S(1)} %stack.30.refs_1_), channel_id=1, source_target_pairs={{0,1},{1,0},{2,3},{3,2},{4,5},{5,4},{6,7},{7,6},{8,9},{9,8},{10,11... | collective-permute-start | bytes 2359304 | tf_op jit(solution)/shard_map/ppermute | solution.py:38
  138.8 14.7 %collective-permute-start.16 = (bf16[128,1536]{1,0:T(8,128)(2,1)S(1)}, bf16[128,1536]{1,0:T(8,128)(2,1)S(1)}, u32[]{:S(2)}, u32[]{:S(2)}) collective-permute-start(bf16[128,1536]{1,0:T(8,128)(2,1)S(1)} %collective-permute-done.14.refs_0_), channel_id=1, source_target_pairs={{0,2},{2,4},{4,6},{6,8},{8,10},{10,12},{12,14},{14,0},{1,3},{3,5},... | collective-permute-start | bytes 1179656 | tf_op jit(solution)/shard_map/ppermute | solution.py:34
  153.5 3.8 %collective-permute-start.19 = (bf16[128,1536]{1,0:T(8,128)(2,1)S(1)}, bf16[128,1536]{1,0:T(8,128)(2,1)S(1)}, u32[]{:S(2)}, u32[]{:S(2)}) collective-permute-start(bf16[128,1536]{1,0:T(8,128)(2,1)S(1)} %collective-permute-done.16.refs_2_), channel_id=1, source_target_pairs={{0,1},{1,0},{2,3},{3,2},{4,5},{5,4},{6,7},{7,6},{8,9},{9,8},{10,11... | collective-permute-start | bytes 1179656 | tf_op jit(solution)/shard_map/ppermute | solution.py:38
  (3 other events, 2.1 us)

commit v2 on v1

--- a/solution.py
+++ b/solution.py
@@ -42,21 +42,25 @@
     return lax.optimization_barrier((*values, *others))[: len(values)]
 
 
-def gathered_y(shard, waits):
+def gathered_y(shard, waits, halves):
     pieces = [shard]
     own, other = [], []
     up = down = shard
     for k in range(4):
         up, down = after((up, down), waits[k]) if waits[k] else (up, down)
+        if k == 3 and halves:
+            middle = shard.shape[0] // 2
+            up, down = up[:middle], down[middle:]
         up = shifted(up, 1)
-        down = shifted(down, -1) if k < 3 else None
+        if k < 3 or halves:
+            down = shifted(down, -1)
         if k in (2, 3):
             own.append(stacked_pieces(pieces) if len(pieces) > 1 else pieces[0])
             other.append(swapped(own[-1]))
             pieces = []
-        pieces += [up, down] if k < 3 else [up]
-    own.append(pieces[0])
-    other.append(swapped(pieces[0]))
+        pieces += [up, down] if k < 3 or halves else [up]
+    own.append(stacked_pieces(pieces) if halves else pieces[0])
+    other.append(swapped(own[-1]))
     return own, other
 
 
@@ -109,7 +113,11 @@
     )(*pieces)
 
 
-def against(a_ref, refs, cols):
+def against(a_refs, refs, cols):
+    return jnp.concatenate([rows_against(a_ref, refs, cols) for a_ref in a_refs], axis=0)
+
+
+def rows_against(a_ref, refs, cols):
     total = None
     first = 0
     for ref in refs:
@@ -151,16 +159,18 @@
         out_ref[rows, j * ROWS : (j + 1) * ROWS] = part.astype(BF16)
 
 
-def normed_tokens(tokens, pre_gain, where):
+def normed_tokens(tokens, pre_gain, where, half):
     rows, width = tokens.shape
-    tile = 128
+    rows = rows // 2
+    tile = 64
+    skip = half * (rows // tile)
     return pl.pallas_call(
         norm_kernel,
         grid_spec=pltpu.PrefetchScalarGridSpec(
             num_scalar_prefetch=1,
             grid=(rows // tile,),
             in_specs=[
-                pl.BlockSpec((tile, width), lambda i, b: (i, 0)),
+                pl.BlockSpec((tile, width), lambda i, b: (i + skip, 0)),
                 pl.BlockSpec((1, width), lambda i, b: (0, 0)),
             ],
             out_specs=pl.BlockSpec(memory_space=pltpu.VMEM),
@@ -168,7 +178,7 @@
         out_shape=jax.ShapeDtypeStruct((rows, width), BF16),
         compiler_params=pltpu.CompilerParams(vmem_limit_bytes=6 << 20),
         name="norm",
-    )(where, in_hbm(tokens), pre_gain.reshape(1, width))
+    )(where, in_hbm(tokens), in_hbm(pre_gain.reshape(1, width)))
 
 
 def vmem_spec():
@@ -179,12 +189,12 @@
     return pltpu.CompilerParams(vmem_limit_bytes=mib << 20)
 
 
-def project_kernel(a_ref, *refs):
+def project_kernel(*refs):
     out_ref = refs[-1]
     seqs, heads, _, local_len, _ = out_ref.shape
     wide = heads * HK
     cols = pl.ds(pl.multiple_of(pl.program_id(0) * wide, wide), wide)
-    total = against(a_ref, refs[:-1], cols).astype(BF16)
+    total = against(refs[:2], refs[2:-1], cols).astype(BF16)
     for n in range(heads):
         out_ref[:, n, 0] = total[:, n * HK : (n + 1) * HK].reshape(seqs, local_len, HK)
 
@@ -194,12 +204,12 @@
     return pl.pallas_call(
         project_kernel,
         grid=(HEADS,),
-        in_specs=[vmem_spec()] * (1 + len(stacks)),
+        in_specs=[vmem_spec()] * (2 + len(stacks)),
         out_specs=pl.BlockSpec(block, lambda j: (0, j % 2, j // 2, 0, 0)),
         out_shape=pltpu.HBM((seqs, HEADS, 2, local_len, HK), BF16),
         compiler_params=limit(8),
         name="project",
-    )(normed, *stacks)
+    )(*normed, *stacks)
 
 
 def pair_masks():
@@ -217,72 +227,87 @@
     return keys, dot(ones, high) + dot(ones, low)
 
 
-def state_kernel(fv_ref, run_ref, tail_ref, gap_ref, state_ref, out_ref, carry_ref):
+def parts_of(a):
+    high = a.astype(BF16).astype(F32)
+    middle = (a - high).astype(BF16).astype(F32)
+    return high, middle, a - high - middle
+
+
+def state_kernel(head_ref, fv_ref, extra_ref, bound_ref, state_ref, out_ref, carry_ref):
     chunks = out_ref.shape[0]
-    causal, first_row, _ = pair_masks()
+    causal, first_row, first_col = pair_masks()
     ones = causal.astype(F32).astype(BF16)
-    gap = gap_ref[...]
+    gap = 1.0 - bound_ref[:, pl.ds(pl.multiple_of(head_ref[0] * HK, HK), HK)]
+    tail_row = lax.broadcasted_iota(jnp.int32, (TAIL, HK), 0)
     block = pl.program_id(0)
 
     @pl.when(block == 0)
     def _():
-        carry_ref[...] = state_ref[...]
+        carry_ref[...] = state_ref[0].T
 
     state = carry_ref[...]
     for p in range(chunks // 2):
         b = block * chunks + 2 * p
         f = fv_ref[pl.ds(b, 2), 0].reshape(PAIR, HK).astype(F32)
         keys, total = keys_and_total(f, gap, ones)
-        run_row = run_ref[pl.ds(block * (chunks // 2) + p, 1), :]
-        run = jnp.broadcast_to(run_row, (PAIR, PAIR)).T
+        lanes = pl.ds(pl.multiple_of(b * CHUNK, PAIR), PAIR)
+        extra = jnp.broadcast_to(extra_ref[:, lanes], (PAIR, PAIR))
+        run_rows = sum(dot_nt(part.astype(BF16), ones) for part in parts_of(extra))
+        run = run_rows.T
         ends = [total[n * CHUNK + CHUNK - 1 : (n + 1) * CHUNK, :] for n in range(2)]
         run_ends = [run[n * CHUNK + CHUNK - 1 : (n + 1) * CHUNK, :] for n in range(2)]
         end = jnp.where(first_row, ends[0], ends[1])
         run_end = jnp.where(first_row, run_ends[0], run_ends[1])
         weighted = (keys * jnp.exp((end - total) + (run_end - run))).astype(BF16)
+        own = run_rows[0:TAIL, :]
+        turned = pltpu.roll(own, CHUNK, 1)
+        first_lane = first_col[0:TAIL, :]
         for n in range(2):
+            both = jnp.where(first_lane, own, turned) if n == 0 else jnp.where(first_lane, turned, own)
+            high, middle, low = parts_of(both)
+            tail = jnp.where(tail_row == 0, high, jnp.where(tail_row == 1, middle, low))
             out_ref[2 * p + n, 0:HV, :] = state.astype(BF16)
-            out_ref[2 * p + n, HV:, :] = tail_ref[b + n]
+            out_ref[2 * p + n, HV:, :] = tail.astype(BF16)
             rows = slice(n * CHUNK, (n + 1) * CHUNK)
             added = dot_tn(fv_ref[b + n, 1], weighted[rows])
             state = state * jnp.exp(ends[n] + run_ends[n]) + added
     carry_ref[...] = state
 
 
-def chunk_states(fv, run, tail, gap, state):
+def chunk_states(fv, extra, bound, state, head):
     chunks = fv.shape[0]
     group = 8
     return pl.pallas_call(
         state_kernel,
         grid=(chunks // group,),
         in_specs=[
+            pl.BlockSpec(memory_space=pltpu.SMEM),
             vmem_spec(),
-            pl.BlockSpec(run.shape, lambda i: (0, 0)),
-            pl.BlockSpec(tail.shape, lambda i: (0, 0, 0)),
-            pl.BlockSpec(gap.shape, lambda i: (0, 0)),
-            pl.BlockSpec(state.shape, lambda i: (0, 0)),
+            pl.BlockSpec(extra.shape, lambda i: (0, 0)),
+            pl.BlockSpec(bound.shape, lambda i: (0, 0)),
+            pl.BlockSpec(state.shape, lambda i: (0, 0, 0)),
         ],
         out_specs=pl.BlockSpec((group, HV + TAIL, HK), lambda i: (i, 0, 0)),
         out_shape=pltpu.HBM((chunks, HV + TAIL, HK), BF16),
         scratch_shapes=[pltpu.VMEM((HV, HK), F32)],
         compiler_params=limit(6),
         name="state",
-    )(fv, in_hbm(run), in_hbm(tail), in_hbm(gap), in_hbm(state))
-
-
-def local_kernel(a_ref, fv_ref, gap_ref, *refs):
-    out_ref, stacks = refs[-1], refs[:-1]
+    )(head, fv, in_hbm(extra), in_hbm(bound), in_hbm(state))
+
+
+def local_kernel(fv_ref, bound_ref, *refs):
+    out_ref, a_refs, stacks = refs[-1], refs[:2], refs[2:-1]
     seqs, heads, _, _, _ = fv_ref.shape
     wide = heads * HK
     causal, _, _ = pair_masks()
     ones = causal.astype(F32).astype(BF16)
-    q_pre = against(a_ref, stacks, slice(0, wide)).astype(BF16)
-    g_pre = against(a_ref, stacks, slice(wide, 2 * wide)).astype(BF16)
+    q_pre = against(a_refs, stacks, slice(0, wide)).astype(BF16)
+    g_pre = against(a_refs, stacks, slice(wide, 2 * wide)).astype(BF16)
     for p in range(seqs // 2):
         for h in range(heads):
             q = q_pre[p * PAIR : (p + 1) * PAIR, h * HK : (h + 1) * HK].astype(F32)
             f = fv_ref[2 * p : 2 * p + 2, h, 0].reshape(PAIR, HK).astype(F32)
-            keys, total = keys_and_total(f, gap_ref[h : h + 1, :], ones)
+            keys, total = keys_and_total(f, 1.0 - bound_ref[:, h * HK : (h + 1) * HK], ones)
             q_scaled = (q * sigmoid(q) * jnp.exp(total)).astype(BF16)
             k_scaled = (keys * jnp.exp(-total)).astype(BF16)
             out_ref[0, p, h] = q_scaled
@@ -302,15 +327,15 @@
             j += 1
 
 
-def local_parts(normed, stacks, fv, gap):
+def local_parts(normed, stacks, fv, bound):
     seqs, heads, _, _, _ = fv.shape
     return pl.pallas_call(
         local_kernel,
-        in_specs=[vmem_spec()] * (3 + len(stacks)),
+        in_specs=[vmem_spec()] * (4 + len(stacks)),
         out_shape=pltpu.HBM((3, seqs // 2, heads, PAIR, HK), BF16),
         compiler_params=limit(14),
         name="local",
-    )(normed, fv, gap, *stacks)
+    )(fv, bound, *normed, *stacks)
 
 
 def out_weight(where, stacks, width):
@@ -396,32 +421,26 @@
     seqs, local_len, width = tokens.shape
     items = seqs * HEADS
     where = jnp.stack([lax.axis_index("y"), lax.axis_index("c")]).astype(jnp.int32)
-    gaps = (1.0 - lower_bound).reshape(HEADS, HK)
+    bound = lower_bound.reshape(1, HEADS * HK)
+    head = lax.axis_index("x").astype(jnp.int32).reshape(1)
 
     first = joined((w_forget, w_value), ((0, (0, 0), (0, 0)), (1, (0, 0), (0, WIDE))), 2 * WIDE)
     places = [(0, (0, 0), (0, 0)), (1, (0, 0), (0, WIDE))]
     places += [(2, (0, n * WIDE), (n * OUT_ROWS, 2 * WIDE)) for n in range(width // WIDE)]
     second = joined((w_query, w_gate, w_out), tuple(places), 3 * WIDE)
-    gap = lax.dynamic_slice_in_dim(gaps, lax.axis_index("x"), 1, 0)
-    run = jnp.cumsum(extra_decay.reshape(items, CHUNK), axis=1)
-    high = lax.reduce_precision(run, 8, 7)
-    middle = lax.reduce_precision(run - high, 8, 7)
-    low = run - high - middle
-    tail = jnp.stack([high, middle, low] + [jnp.zeros_like(high)] * (TAIL - 3), axis=1)
-    tail = jnp.concatenate([tail, tail], axis=2).astype(BF16)
-    run = run.reshape(items // 2, PAIR)
-    state = initial_state[0].T
-    normed = normed_tokens(tokens.reshape(seqs * local_len, width), pre_gain, where)
-
-    first_own, first_other = gathered_y(first, ((), (normed,), (second,), ()))
+    rows = tokens.reshape(seqs * local_len, width)
+    normed = [normed_tokens(rows, pre_gain, where, half) for half in range(2)]
+
+    first_own, first_other = gathered_y(first, ((), normed[:1], normed[1:], (second,)), True)
     fv = project_heads(normed, first_own + first_other, seqs, local_len)
     moved = lax.all_to_all(fv.reshape(items, 2 * local_len, HK), SP, 0, 0, tiled=True)
-    starts = chunk_states(moved.reshape(items, 2, local_len, HK), run, tail, gap, state)
+    moved = moved.reshape(items, 2, local_len, HK)
+    starts = chunk_states(moved, extra_decay, bound, initial_state, head)
     states = lax.all_to_all(starts, SP, 0, 0, tiled=True)
 
-    second_own, second_other = gathered_y(second, ((), (), (), ()))
+    second_own, second_other = gathered_y(second, ((), (), (), ()), False)
     stacks = second_own + second_other
-    parts = local_parts(normed, stacks, fv, gaps)
+    parts = local_parts(normed, stacks, fv, bound)
     weight = out_weight(where, stacks, width)
     states = states.reshape(seqs, HEADS, HV + TAIL, HK)
     return output_rows(states, parts, fv, weight, norm_gain, post_gain)

time: 171 us -> 178 us (1.041)
  waiting for transfers between devices: 39.8 us -> 52.2 us
  local copies, waits for them, and re-layouts: 8.17 us -> 0.04 us
  Pallas kernels: 27.5 us -> 34 us
  other arithmetic: 5.97 us -> 0.08 us
  starting transfers between devices: 87.3 us -> 89.8 us
    all_to_all x1, waiting for transfers between devices: 0.01 us -> 8.96 us  [layer(): lax.all_to_all(fv.reshape(items, 2 * local_len, HK), SP, 0, 0, tiled=True)]
    pallas_call x3, Pallas kernels: 13.7 us -> 17.7 us  [the longest x1 8.12 us: chunk_states(): pl.pallas_call(state_kernel, grid=(chunks // group,), in_specs=[pl.BlockS...]
    ppermute x14 -> x15, waiting for transfers between devices: 37.4 us -> 40.7 us  [shifted(): return lax.ppermute(a, 'y', [(i, (i + step) % size) for i in range(size)])]
    all_to_all x1, starting transfers between devices: 9.33 us -> 6.47 us  [layer(): states = lax.all_to_all(starts, SP, 0, 0, tiled=True)]
    another operation x3 -> x0, local copies, waits for them, and re-layouts: 2.79 us -> none  [layer(): jnp.stack([high, middle, low] + [jnp.zeros_like(high)] * (TAIL - 3), axis=1)]
    unnamed x12 -> x8, local copies, waits for them, and re-layouts: 2.79 us -> 0.02 us
    ppermute x14 -> x15, starting transfers between devices: 45.2 us -> 47.8 us  [shifted(): return lax.ppermute(a, 'y', [(i, (i + step) % size) for i in range(size)])]
    pallas_call x1 -> x2, Pallas kernels: 3.58 us -> 6.07 us  [normed_tokens(): pl.pallas_call(norm_kernel, grid_spec=pltpu.PrefetchScalarGridSpec(num_sc...]
  transfers between devices with their start and end apart: 22 -> 23, of which waited for: 9 -> 13; matrix products, arithmetic and copies ran while one was open for 8% -> 0% of each run, Pallas kernels for 10% -> 13%
where the time goes in v2:
time: 178 us; the launch traced here: 176 us
  starting transfers between devices  89.8 us (50%)
  waiting for transfers between devices  52.2 us (29%)
  Pallas kernels  34 us (19%)
    ppermute x15, starting transfers between devices, shifted(): return lax.ppermute(a, 'y', [(i, (i + step) % size) for i in range(size)])  47.8 us
    ppermute x15, waiting for transfers between devices, shifted(): return lax.ppermute(a, 'y', [(i, (i + step) % size) for i in range(size)])  40.7 us
    ppermute x6, starting transfers between devices, swapped(): return lax.ppermute(a, 'c', [(0, 1), (1, 0)])  23 us
    all_to_all x1, starting transfers between devices, layer(): lax.all_to_all(fv.reshape(items, 2 * local_len, HK), SP, 0, 0, tiled=True)  12.7 us
    all_to_all x1, waiting for transfers between devices, layer(): lax.all_to_all(fv.reshape(items, 2 * local_len, HK), SP, 0, 0, tiled=True)  8.96 us
    pallas_call x1, Pallas kernels, chunk_states(): pl.pallas_call(state_kernel, grid=(chunks // group,), in_specs=[pl.BlockS...  8.12 us
    all_to_all x1, starting transfers between devices, layer(): states = lax.all_to_all(starts, SP, 0, 0, tiled=True)  6.47 us
    pallas_call x2, Pallas kernels, normed_tokens(): pl.pallas_call(norm_kernel, grid_spec=pltpu.PrefetchScalarGridSpec(num_sc...  6.07 us
  transfers between devices with their start and end apart: 23, of which 13 were waited for; matrix products, arithmetic and copies ran while one was open for 0% of the time, Pallas kernels for 13%

profile of v2, /device:TPU:1, one launch (start us, length us, event | category | flops | bytes accessed | tf_op | source)
XLA Modules:
  0.0 176.5 jit_solution(18417503338350585242)
XLA Ops:
  1.0 5.9 %collective-permute-start.1 = (bf16[128,1024]{1,0:T(8,128)(2,1)S(1)}, bf16[128,1024]{1,0:T(8,128)(2,1)S(1)}, u32[]{:S(2)}, u32[]{:S(2)}) collective-permute-start(bf16[128,1024]{1,0:T(8,128)(2,1)S(1)} %shard_map.118.refs_0_), channel_id=1, source_target_pairs={{0,14},{2,0},{4,2},{6,4},{8,6},{10,8},{12,10},{14,12},{1,15},{3,1}... | collective-permute-start | bytes 786440 | tf_op jit(solution)/shard_map/ppermute | solution.py:34
  12.0 3.3 %collective-permute-done.refs_1_ = bf16[128,1024]{1,0:T(8,128)(2,1)S(1)} collective-permute-done((bf16[128,1024]{1,0:T(8,128)(2,1)S(1)}, bf16[128,1024]{1,0:T(8,128)(2,1)S(1)}, u32[]{:S(2)}, u32[]{:S(2)}) %collective-permute-start) | collective-permute-done | bytes 262176 | tf_op jit(solution)/shard_map/ppermute | solution.py:34
  17.2 4.6 %collective-permute-start.3 = (bf16[128,1024]{1,0:T(8,128)(2,1)S(1)}, bf16[128,1024]{1,0:T(8,128)(2,1)S(1)}, u32[]{:S(2)}, u32[]{:S(2)}) collective-permute-start(bf16[128,1024]{1,0:T(8,128)(2,1)S(1)} %collective-permute-done.1.refs_2_), channel_id=1, source_target_pairs={{0,14},{2,0},{4,2},{6,4},{8,6},{10,8},{12,10},{14,12},{1,15},{3,1}... | collective-permute-start | bytes 786440 | tf_op jit(solution)/shard_map/ppermute | solution.py:34
  25.1 7.1 %collective-permute-start.8 = (bf16[640,1024]{1,0:T(8,128)(2,1)S(1)}, bf16[640,1024]{1,0:T(8,128)(2,1)S(1)}, u32[]{:S(2)}, u32[]{:S(2)}) collective-permute-start(bf16[640,1024]{1,0:T(8,128)(2,1)S(1)} %stack.17.refs_2_), channel_id=1, source_target_pairs={{0,1},{1,0},{2,3},{3,2},{4,5},{5,4},{6,7},{7,6},{8,9},{9,8},{10,11... | collective-permute-start | bytes 3932168 | tf_op jit(solution)/shard_map/ppermute | solution.py:38
  37.2 5.3 %collective-permute-start.5 = (bf16[128,1024]{1,0:T(8,128)(2,1)S(1)}, bf16[128,1024]{1,0:T(8,128)(2,1)S(1)}, u32[]{:S(2)}, u32[]{:S(2)}) collective-permute-start(bf16[128,1024]{1,0:T(8,128)(2,1)S(1)} %collective-permute-done.3.refs_4_), channel_id=1, source_target_pairs={{0,14},{2,0},{4,2},{6,4},{8,6},{10,8},{12,10},{14,12},{1,15},{3,1}... | collective-permute-start | bytes 786440 | tf_op jit(solution)/shard_map/ppermute | solution.py:34
  42.5 4.7 %collective-permute-done.4.refs_0_ = bf16[128,1024]{1,0:T(8,128)(2,1)S(1)} collective-permute-done((bf16[128,1024]{1,0:T(8,128)(2,1)S(1)}, bf16[128,1024]{1,0:T(8,128)(2,1)S(1)}, u32[]{:S(2)}, u32[]{:S(2)}) %collective-permute-start.4) | collective-permute-done | bytes 262176 | tf_op jit(solution)/shard_map/ppermute | solution.py:34
  52.0 5.3 %collective-permute-start.7 = (bf16[64,1024]{1,0:T(8,128)(2,1)S(1)}, bf16[64,1024]{1,0:T(8,128)(2,1)S(1)}, u32[]{:S(2)}, u32[]{:S(2)}) collective-permute-start(bf16[64,1024]{1,0:T(8,128)(2,1)S(1)} %slice.7), channel_id=1, source_target_pairs={{0,14},{2,0},{4,2},{6,4},{8,6},{10,8},{12,10},{14,12},{1,15},{3,1}... | collective-permute-start | bytes 393224 | tf_op jit(solution)/shard_map/ppermute | solution.py:34
  60.1 5.0 %collective-permute-done.6.refs_0_ = bf16[64,1024]{1,0:T(8,128)(2,1)S(1)} collective-permute-done((bf16[64,1024]{1,0:T(8,128)(2,1)S(1)}, bf16[64,1024]{1,0:T(8,128)(2,1)S(1)}, u32[]{:S(2)}, u32[]{:S(2)}) %collective-permute-start.6) | collective-permute-done | bytes 131104 | tf_op jit(solution)/shard_map/ppermute | solution.py:34
  65.2 3.1 %collective-permute-start.10 = (bf16[128,1024]{1,0:T(8,128)(2,1)S(1)}, bf16[128,1024]{1,0:T(8,128)(2,1)S(1)}, u32[]{:S(2)}, u32[]{:S(2)}) collective-permute-start(bf16[128,1024]{1,0:T(8,128)(2,1)S(1)} %stack.19.refs_4_), channel_id=1, source_target_pairs={{0,1},{1,0},{2,3},{3,2},{4,5},{5,4},{6,7},{7,6},{8,9},{9,8},{10,11... | collective-permute-start | bytes 786440 | tf_op jit(solution)/shard_map/ppermute | solution.py:38
  69.4 4.2 %project.1.fv_ref = bf16[8,4,2,64,128]{4,3,2,1,0:T(8,128)(2,1)} custom-call(bf16[256,2048]{1,0:T(8,128)(2,1)S(1)} %norm.2.refs_0_, bf16[256,2048]{1,0:T(8,128)(2,1)S(1)} %norm.3.refs_1_, bf16[640,1024]{1,0:T(8,128)(2,1)S(1)} %stack.17.refs_2_, bf16[256,1024]{1,0:T(8,128)(2,1)S(1)} %stack.18.refs_3_, bf16[128,1024]{1,0:T(8,128)(2,1)S(1)} %stack.19.refs_4_, ...), custom_call_target="tpu_custom_call" | custom-call | tf_op jit(solution)/shard_map/project/pallas_call | solution.py:204
  73.7 12.7 %all-to-all-start = ((bf16[32,128,128]{2,1,0:T(8,128)(2,1)}), bf16[32,128,128]{2,1,0:T(8,128)(2,1)S(1)}, u32[]{:S(2)}, u32[]{:S(2)}) async-start(bf16[32,128,128]{2,1,0:T(8,128)(2,1)} %bitcast.11), calls=%async_computation | async-start | bytes 2097152 | tf_op jit(solution)/shard_map/all_to_all | solution.py:436
  88.3 3.4 %collective-permute-start.11 = (bf16[128,1536]{1,0:T(8,128)(2,1)S(1)}, bf16[128,1536]{1,0:T(8,128)(2,1)}, u32[]{:S(2)}, u32[]{:S(2)}) collective-permute-start(bf16[128,1536]{1,0:T(8,128)(2,1)S(1)} %shard_map.119.refs_0_), channel_id=1, source_target_pairs={{0,2},{2,4},{4,6},{6,8},{8,10},{10,12},{12,14},{14,0},{1,3},{3,5},... | collective-permute-start | bytes 1179656 | tf_op jit(solution)/shard_map/ppermute | solution.py:34
  91.6 6.7 %collective-permute-done.12.refs_2_ = bf16[128,1536]{1,0:T(8,128)(2,1)} collective-permute-done((bf16[128,1536]{1,0:T(8,128)(2,1)S(1)}, bf16[128,1536]{1,0:T(8,128)(2,1)}, u32[]{:S(2)}, u32[]{:S(2)}) %collective-permute-start.12) | collective-permute-done | bytes 393248 | tf_op jit(solution)/shard_map/ppermute | solution.py:34
  98.3 3.4 %collective-permute-start.14 = (bf16[128,1536]{1,0:T(8,128)(2,1)}, bf16[128,1536]{1,0:T(8,128)(2,1)}, u32[]{:S(2)}, u32[]{:S(2)}) collective-permute-start(bf16[128,1536]{1,0:T(8,128)(2,1)} %collective-permute-done.12.refs_2_), channel_id=1, source_target_pairs={{0,14},{2,0},{4,2},{6,4},{8,6},{10,8},{12,10},{14,12},{1,15},{3,1}... | collective-permute-start | bytes 1179656 | tf_op jit(solution)/shard_map/ppermute | solution.py:34
  103.7 9.0 %all-to-all-done = bf16[32,128,128]{2,1,0:T(8,128)(2,1)S(1)} async-done(((bf16[32,128,128]{2,1,0:T(8,128)(2,1)}), bf16[32,128,128]{2,1,0:T(8,128)(2,1)S(1)}, u32[]{:S(2)}, u32[]{:S(2)}) %all-to-all-start) | async-done | bytes 1048608 | tf_op jit(solution)/shard_map/all_to_all | solution.py:436
  112.6 8.1 %state.1 = bf16[32,136,128]{2,1,0:T(8,128)(2,1)} custom-call(s32[1]{0:T(128)} %bitcast.head_ref, bf16[32,2,64,128]{3,2,1,0:T(8,128)(2,1)S(1)} %bitcast.12, f32[1,2048]{1,0:T(1,128)} %extra_ref.1, f32[1,512]{1,0:T(1,128)} %bitcast.14, f32[1,128,128]{2,1,0:T(8,128)} %state_ref.1), custom_call_target="tpu_custom_call" | custom-call | tf_op jit(solution)/shard_map/state/pallas_call | solution.py:280
  120.7 6.5 %all-to-all-start.1 = ((bf16[32,136,128]{2,1,0:T(8,128)(2,1)}), bf16[32,136,128]{2,1,0:T(8,128)(2,1)}, u32[]{:S(2)}, u32[]{:S(2)}) async-start(bf16[32,136,128]{2,1,0:T(8,128)(2,1)} %state.1), calls=%async_computation.1 | async-start | bytes 2228224 | tf_op jit(solution)/shard_map/all_to_all | solution.py:439
  128.8 3.8 %collective-permute-start.18 = (bf16[640,1536]{1,0:T(8,128)(2,1)S(1)}, bf16[640,1536]{1,0:T(8,128)(2,1)S(1)}, u32[]{:S(2)}, u32[]{:S(2)}) collective-permute-start(bf16[640,1536]{1,0:T(8,128)(2,1)S(1)} %stack.20.refs_2_.refs_0_), channel_id=1, source_target_pairs={{0,1},{1,0},{2,3},{3,2},{4,5},{5,4},{6,7},{7,6},{8,9},{9,8},{10,11... | collective-permute-start | bytes 5898248 | tf_op jit(solution)/shard_map/ppermute | solution.py:38
  134.6 4.6 %collective-permute-start.16 = (bf16[128,1536]{1,0:T(8,128)(2,1)}, bf16[128,1536]{1,0:T(8,128)(2,1)S(1)}, u32[]{:S(2)}, u32[]{:S(2)}) collective-permute-start(bf16[128,1536]{1,0:T(8,128)(2,1)} %collective-permute-done.14.refs_4_), channel_id=1, source_target_pairs={{0,14},{2,0},{4,2},{6,4},{8,6},{10,8},{12,10},{14,12},{1,15},{3,1}... | collective-permute-start | bytes 1179656 | tf_op jit(solution)/shard_map/ppermute | solution.py:34
  139.2 7.6 %collective-permute-done.15.refs_0_ = bf16[128,1536]{1,0:T(8,128)(2,1)S(1)} collective-permute-done((bf16[128,1536]{1,0:T(8,128)(2,1)}, bf16[128,1536]{1,0:T(8,128)(2,1)S(1)}, u32[]{:S(2)}, u32[]{:S(2)}) %collective-permute-start.15) | collective-permute-done | bytes 393248 | tf_op jit(solution)/shard_map/ppermute | solution.py:34
  151.4 8.3 %collective-permute-done.17.refs_4_.refs_2_ = bf16[128,1536]{1,0:T(8,128)(2,1)S(1)} collective-permute-done((bf16[128,1536]{1,0:T(8,128)(2,1)S(1)}, bf16[128,1536]{1,0:T(8,128)(2,1)S(1)}, u32[]{:S(2)}, u32[]{:S(2)}) %collective-permute-start.17) | collective-permute-done | bytes 393248 | tf_op jit(solution)/shard_map/ppermute | solution.py:34
  159.8 3.5 %collective-permute-start.20 = (bf16[128,1536]{1,0:T(8,128)(2,1)S(1)}, bf16[128,1536]{1,0:T(8,128)(2,1)S(1)}, u32[]{:S(2)}, u32[]{:S(2)}) collective-permute-start(bf16[128,1536]{1,0:T(8,128)(2,1)S(1)} %collective-permute-done.17.refs_4_.refs_2_), channel_id=1, source_target_pairs={{0,1},{1,0},{2,3},{3,2},{4,5},{5,4},{6,7},{7,6},{8,9},{9,8},{10,11... | collective-permute-start | bytes 1179656 | tf_op jit(solution)/shard_map/ppermute | solution.py:38
  164.6 5.3 %local.1.part_ref = bf16[3,4,4,128,128]{4,3,2,1,0:T(8,128)(2,1)} custom-call(bf16[8,4,2,64,128]{4,3,2,1,0:T(8,128)(2,1)S(1)} %copy-done, f32[1,512]{1,0:T(1,128)S(1)} %bitcast.15, bf16[256,2048]{1,0:T(8,128)(2,1)S(1)} %norm.2.refs_0_, bf16[256,2048]{1,0:T(8,128)(2,1)S(1)} %norm.3.refs_1_, bf16[640,1536]{1,0:T(8,128)(2,1)S(1)} %stack.20.refs_2_.refs_0_, ...), custom_call_target="tpu_custom_call" | custom-call | tf_op jit(solution)/shard_map/local/pallas_call | solution.py:332
  170.7 5.8 %output.1 = bf16[8,64,2048]{2,1,0:T(8,128)(2,1)} custom-call(bf16[8,4,136,128]{3,2,1,0:T(8,128)(2,1)} %bitcast.8.state_ref, bf16[3,4,4,128,128]{4,3,2,1,0:T(8,128)(2,1)} %local.1.part_ref, bf16[8,4,2,64,128]{4,3,2,1,0:T(8,128)(2,1)} %project.1.fv_ref, bf16[512,2048]{1,0:T(8,128)(2,1)S(1)} %weight.1.weight_ref, f32[1,128]{1,0:T(1,128)S(1)} %bitcast.16, ...), custom_call_target="tpu_custom_call" | custom-call | tf_op jit(solution)/shard_map/output/pallas_call | solution.py:389
  (47 shorter events, 39.0 us)
Async XLA Ops:
  1.0 11.0 %collective-permute-start.1 = (bf16[128,1024]{1,0:T(8,128)(2,1)S(1)}, bf16[128,1024]{1,0:T(8,128)(2,1)S(1)}, u32[]{:S(2)}, u32[]{:S(2)}) collective-permute-start(bf16[128,1024]{1,0:T(8,128)(2,1)S(1)} %shard_map.118.refs_0_), channel_id=1, source_target_pairs={{0,14},{2,0},{4,2},{6,4},{8,6},{10,8},{12,10},{14,12},{1,15},{3,1}... | collective-permute-start | bytes 786440 | tf_op jit(solution)/shard_map/ppermute | solution.py:34
  6.9 8.3 %collective-permute-start = (bf16[128,1024]{1,0:T(8,128)(2,1)S(1)}, bf16[128,1024]{1,0:T(8,128)(2,1)S(1)}, u32[]{:S(2)}, u32[]{:S(2)}) collective-permute-start(bf16[128,1024]{1,0:T(8,128)(2,1)S(1)} %shard_map.118.refs_0_), channel_id=1, source_target_pairs={{0,2},{2,4},{4,6},{6,8},{8,10},{10,12},{12,14},{14,0},{1,3},{3,5},... | collective-permute-start | bytes 786440 | tf_op jit(solution)/shard_map/ppermute | solution.py:34
  15.2 8.3 %collective-permute-start.2 = (bf16[128,1024]{1,0:T(8,128)(2,1)S(1)}, bf16[128,1024]{1,0:T(8,128)(2,1)S(1)}, u32[]{:S(2)}, u32[]{:S(2)}) collective-permute-start(bf16[128,1024]{1,0:T(8,128)(2,1)S(1)} %collective-permute-done.refs_1_), channel_id=1, source_target_pairs={{0,2},{2,4},{4,6},{6,8},{8,10},{10,12},{12,14},{14,0},{1,3},{3,5},... | collective-permute-start | bytes 786440 | tf_op jit(solution)/shard_map/ppermute | solution.py:34
  17.2 7.9 %collective-permute-start.3 = (bf16[128,1024]{1,0:T(8,128)(2,1)S(1)}, bf16[128,1024]{1,0:T(8,128)(2,1)S(1)}, u32[]{:S(2)}, u32[]{:S(2)}) collective-permute-start(bf16[128,1024]{1,0:T(8,128)(2,1)S(1)} %collective-permute-done.1.refs_2_), channel_id=1, source_target_pairs={{0,14},{2,0},{4,2},{6,4},{8,6},{10,8},{12,10},{14,12},{1,15},{3,1}... | collective-permute-start | bytes 786440 | tf_op jit(solution)/shard_map/ppermute | solution.py:34
  25.1 44.3 %collective-permute-start.8 = (bf16[640,1024]{1,0:T(8,128)(2,1)S(1)}, bf16[640,1024]{1,0:T(8,128)(2,1)S(1)}, u32[]{:S(2)}, u32[]{:S(2)}) collective-permute-start(bf16[640,1024]{1,0:T(8,128)(2,1)S(1)} %stack.17.refs_2_), channel_id=1, source_target_pairs={{0,1},{1,0},{2,3},{3,2},{4,5},{5,4},{6,7},{7,6},{8,9},{9,8},{10,11... | collective-permute-start | bytes 3932168 | tf_op jit(solution)/shard_map/ppermute | solution.py:38
  35.3 11.9 %collective-permute-start.4 = (bf16[128,1024]{1,0:T(8,128)(2,1)S(1)}, bf16[128,1024]{1,0:T(8,128)(2,1)S(1)}, u32[]{:S(2)}, u32[]{:S(2)}) collective-permute-start(bf16[128,1024]{1,0:T(8,128)(2,1)S(1)} %collective-permute-done.2.refs_3_), channel_id=1, source_target_pairs={{0,2},{2,4},{4,6},{6,8},{8,10},{10,12},{12,14},{14,0},{1,3},{3,5},... | collective-permute-start | bytes 786440 | tf_op jit(solution)/shard_map/ppermute | solution.py:34
  37.2 10.9 %collective-permute-start.5 = (bf16[128,1024]{1,0:T(8,128)(2,1)S(1)}, bf16[128,1024]{1,0:T(8,128)(2,1)S(1)}, u32[]{:S(2)}, u32[]{:S(2)}) collective-permute-start(bf16[128,1024]{1,0:T(8,128)(2,1)S(1)} %collective-permute-done.3.refs_4_), channel_id=1, source_target_pairs={{0,14},{2,0},{4,2},{6,4},{8,6},{10,8},{12,10},{14,12},{1,15},{3,1}... | collective-permute-start | bytes 786440 | tf_op jit(solution)/shard_map/ppermute | solution.py:34
  48.1 21.3 %collective-permute-start.9 = (bf16[256,1024]{1,0:T(8,128)(2,1)S(1)}, bf16[256,1024]{1,0:T(8,128)(2,1)S(1)}, u32[]{:S(2)}, u32[]{:S(2)}) collective-permute-start(bf16[256,1024]{1,0:T(8,128)(2,1)S(1)} %stack.18.refs_3_), channel_id=1, source_target_pairs={{0,1},{1,0},{2,3},{3,2},{4,5},{5,4},{6,7},{7,6},{8,9},{9,8},{10,11... | collective-permute-start | bytes 1572872 | tf_op jit(solution)/shard_map/ppermute | solution.py:38
  52.0 8.1 %collective-permute-start.7 = (bf16[64,1024]{1,0:T(8,128)(2,1)S(1)}, bf16[64,1024]{1,0:T(8,128)(2,1)S(1)}, u32[]{:S(2)}, u32[]{:S(2)}) collective-permute-start(bf16[64,1024]{1,0:T(8,128)(2,1)S(1)} %slice.7), channel_id=1, source_target_pairs={{0,14},{2,0},{4,2},{6,4},{8,6},{10,8},{12,10},{14,12},{1,15},{3,1}... | collective-permute-start | bytes 393224 | tf_op jit(solution)/shard_map/ppermute | solution.py:34
  57.3 7.9 %collective-permute-start.6 = (bf16[64,1024]{1,0:T(8,128)(2,1)S(1)}, bf16[64,1024]{1,0:T(8,128)(2,1)S(1)}, u32[]{:S(2)}, u32[]{:S(2)}) collective-permute-start(bf16[64,1024]{1,0:T(8,128)(2,1)S(1)} %slice.6), channel_id=1, source_target_pairs={{0,2},{2,4},{4,6},{6,8},{8,10},{10,12},{12,14},{14,0},{1,3},{3,5},... | collective-permute-start | bytes 393224 | tf_op jit(solution)/shard_map/ppermute | solution.py:34
  65.2 4.2 %collective-permute-start.10 = (bf16[128,1024]{1,0:T(8,128)(2,1)S(1)}, bf16[128,1024]{1,0:T(8,128)(2,1)S(1)}, u32[]{:S(2)}, u32[]{:S(2)}) collective-permute-start(bf16[128,1024]{1,0:T(8,128)(2,1)S(1)} %stack.19.refs_4_), channel_id=1, source_target_pairs={{0,1},{1,0},{2,3},{3,2},{4,5},{5,4},{6,7},{7,6},{8,9},{9,8},{10,11... | collective-permute-start | bytes 786440 | tf_op jit(solution)/shard_map/ppermute | solution.py:38
  73.7 39.0 %all-to-all-start = ((bf16[32,128,128]{2,1,0:T(8,128)(2,1)}), bf16[32,128,128]{2,1,0:T(8,128)(2,1)S(1)}, u32[]{:S(2)}, u32[]{:S(2)}) async-start(bf16[32,128,128]{2,1,0:T(8,128)(2,1)} %bitcast.11), calls=%async_computation | async-start | bytes 2097152 | tf_op jit(solution)/shard_map/all_to_all | solution.py:436
  86.3 12.0 %collective-permute-start.12 = (bf16[128,1536]{1,0:T(8,128)(2,1)S(1)}, bf16[128,1536]{1,0:T(8,128)(2,1)}, u32[]{:S(2)}, u32[]{:S(2)}) collective-permute-start(bf16[128,1536]{1,0:T(8,128)(2,1)S(1)} %shard_map.119.refs_0_), channel_id=1, source_target_pairs={{0,14},{2,0},{4,2},{6,4},{8,6},{10,8},{12,10},{14,12},{1,15},{3,1}... | collective-permute-start | bytes 1179656 | tf_op jit(solution)/shard_map/ppermute | solution.py:34
  88.3 13.5 %collective-permute-start.11 = (bf16[128,1536]{1,0:T(8,128)(2,1)S(1)}, bf16[128,1536]{1,0:T(8,128)(2,1)}, u32[]{:S(2)}, u32[]{:S(2)}) collective-permute-start(bf16[128,1536]{1,0:T(8,128)(2,1)S(1)} %shard_map.119.refs_0_), channel_id=1, source_target_pairs={{0,2},{2,4},{4,6},{6,8},{8,10},{10,12},{12,14},{14,0},{1,3},{3,5},... | collective-permute-start | bytes 1179656 | tf_op jit(solution)/shard_map/ppermute | solution.py:34
  98.3 28.9 %collective-permute-start.14 = (bf16[128,1536]{1,0:T(8,128)(2,1)}, bf16[128,1536]{1,0:T(8,128)(2,1)}, u32[]{:S(2)}, u32[]{:S(2)}) collective-permute-start(bf16[128,1536]{1,0:T(8,128)(2,1)} %collective-permute-done.12.refs_2_), channel_id=1, source_target_pairs={{0,14},{2,0},{4,2},{6,4},{8,6},{10,8},{12,10},{14,12},{1,15},{3,1}... | collective-permute-start | bytes 1179656 | tf_op jit(solution)/shard_map/ppermute | solution.py:34
  101.7 25.5 %collective-permute-start.13 = (bf16[128,1536]{1,0:T(8,128)(2,1)}, bf16[128,1536]{1,0:T(8,128)(2,1)}, u32[]{:S(2)}, u32[]{:S(2)}) collective-permute-start(bf16[128,1536]{1,0:T(8,128)(2,1)} %collective-permute-done.11.refs_1_), channel_id=1, source_target_pairs={{0,2},{2,4},{4,6},{6,8},{8,10},{10,12},{12,14},{14,0},{1,3},{3,5},... | collective-permute-start | bytes 1179656 | tf_op jit(solution)/shard_map/ppermute | solution.py:34
  120.7 49.9 %all-to-all-start.1 = ((bf16[32,136,128]{2,1,0:T(8,128)(2,1)}), bf16[32,136,128]{2,1,0:T(8,128)(2,1)}, u32[]{:S(2)}, u32[]{:S(2)}) async-start(bf16[32,136,128]{2,1,0:T(8,128)(2,1)} %state.1), calls=%async_computation.1 | async-start | bytes 2228224 | tf_op jit(solution)/shard_map/all_to_all | solution.py:439
  127.2 37.4 %copy-start = (bf16[8,4,2,64,128]{4,3,2,1,0:T(8,128)(2,1)S(1)}, bf16[8,4,2,64,128]{4,3,2,1,0:T(8,128)(2,1)}, u32[]{:S(2)}) copy-start(bf16[8,4,2,64,128]{4,3,2,1,0:T(8,128)(2,1)} %project.1.fv_ref) | copy-start | bytes 3145732
  128.8 35.8 %collective-permute-start.18 = (bf16[640,1536]{1,0:T(8,128)(2,1)S(1)}, bf16[640,1536]{1,0:T(8,128)(2,1)S(1)}, u32[]{:S(2)}, u32[]{:S(2)}) collective-permute-start(bf16[640,1536]{1,0:T(8,128)(2,1)S(1)} %stack.20.refs_2_.refs_0_), channel_id=1, source_target_pairs={{0,1},{1,0},{2,3},{3,2},{4,5},{5,4},{6,7},{7,6},{8,9},{9,8},{10,11... | collective-permute-start | bytes 5898248 | tf_op jit(solution)/shard_map/ppermute | solution.py:38
  132.7 14.1 %collective-permute-start.15 = (bf16[128,1536]{1,0:T(8,128)(2,1)}, bf16[128,1536]{1,0:T(8,128)(2,1)S(1)}, u32[]{:S(2)}, u32[]{:S(2)}) collective-permute-start(bf16[128,1536]{1,0:T(8,128)(2,1)} %collective-permute-done.13.refs_3_), channel_id=1, source_target_pairs={{0,2},{2,4},{4,6},{6,8},{8,10},{10,12},{12,14},{14,0},{1,3},{3,5},... | collective-permute-start | bytes 1179656 | tf_op jit(solution)/shard_map/ppermute | solution.py:34
  134.6 14.1 %collective-permute-start.16 = (bf16[128,1536]{1,0:T(8,128)(2,1)}, bf16[128,1536]{1,0:T(8,128)(2,1)S(1)}, u32[]{:S(2)}, u32[]{:S(2)}) collective-permute-start(bf16[128,1536]{1,0:T(8,128)(2,1)} %collective-permute-done.14.refs_4_), channel_id=1, source_target_pairs={{0,14},{2,0},{4,2},{6,4},{8,6},{10,8},{12,10},{14,12},{1,15},{3,1}... | collective-permute-start | bytes 1179656 | tf_op jit(solution)/shard_map/ppermute | solution.py:34
  146.8 13.0 %collective-permute-start.17 = (bf16[128,1536]{1,0:T(8,128)(2,1)S(1)}, bf16[128,1536]{1,0:T(8,128)(2,1)S(1)}, u32[]{:S(2)}, u32[]{:S(2)}) collective-permute-start(bf16[128,1536]{1,0:T(8,128)(2,1)S(1)} %collective-permute-done.15.refs_0_), channel_id=1, source_target_pairs={{0,2},{2,4},{4,6},{6,8},{8,10},{10,12},{12,14},{14,0},{1,3},{3,5},... | collective-permute-start | bytes 1179656 | tf_op jit(solution)/shard_map/ppermute | solution.py:34
  148.7 15.9 %collective-permute-start.19 = (bf16[256,1536]{1,0:T(8,128)(2,1)S(1)}, bf16[256,1536]{1,0:T(8,128)(2,1)S(1)}, u32[]{:S(2)}, u32[]{:S(2)}) collective-permute-start(bf16[256,1536]{1,0:T(8,128)(2,1)S(1)} %stack.21.refs_3_.refs_1_), channel_id=1, source_target_pairs={{0,1},{1,0},{2,3},{3,2},{4,5},{5,4},{6,7},{7,6},{8,9},{9,8},{10,11... | collective-permute-start | bytes 2359304 | tf_op jit(solution)/shard_map/ppermute | solution.py:38
  159.8 4.9 %collective-permute-start.20 = (bf16[128,1536]{1,0:T(8,128)(2,1)S(1)}, bf16[128,1536]{1,0:T(8,128)(2,1)S(1)}, u32[]{:S(2)}, u32[]{:S(2)}) collective-permute-start(bf16[128,1536]{1,0:T(8,128)(2,1)S(1)} %collective-permute-done.17.refs_4_.refs_2_), channel_id=1, source_target_pairs={{0,1},{1,0},{2,3},{3,2},{4,5},{5,4},{6,7},{7,6},{8,9},{9,8},{10,11... | collective-permute-start | bytes 1179656 | tf_op jit(solution)/shard_map/ppermute | solution.py:38
  (3 other events, 38.8 us)
